TPU v7x, 32 devices: a whole 2x2x4 slice. The times are simulated.
32 devices in a mesh: grp: 2 (over y), fs: 4 (over z), tp: 4 (over x, core).
Axes of the slice: x: 2, y: 2, z: 4, core: 2. Of those that a mesh axis runs over, the one named last changes fastest.
Arguments:
- block_source_tensor: bfloat16 [4096, 2048], P(('grp', 'fs'), 'tp'), parts along dimension 0, may hold values from -6 to 6
- attend_initial_norm_gain: float32 [2048], replicated, may hold values from 0.1 to 1.9
- each_channel_group_norm: float32 [8, 256], P('tp'), may hold values from 0.1 to 1.9
- attend_final_norm_gain: float32 [2048], replicated, may hold values from 0.1 to 1.9
- dense_initial_norm_gain: float32 [2048], replicated, may hold values from 0.1 to 1.9
- dense_final_norm_gain: float32 [2048], replicated, may hold values from 0.1 to 1.9
- question_map: bfloat16 [2048, 1024], P('fs', 'tp'), may hold values from -0.125 to 0.125
- address_map: bfloat16 [2048, 1024], P('fs', 'tp'), may hold values from -0.125 to 0.125
- payload_weights_map: bfloat16 [2048, 2048], P('fs', 'tp'), may hold values from -0.125 to 0.125
- fading_left_factor: bfloat16 [2048, 16], replicated, may hold values from -0.125 to 0.125
- fading_right_factor: float32 [16, 1024], P(None, 'tp'), may hold values from -1.5 to 1.5
- fading_valve_constant: float32 [1024], P('tp'), may hold values from 0.05 to 6.2
- sudden_fade_excess: float32 [4096, 1024], P(('grp', 'fs'), 'tp'), parts along dimension 0, may hold values from -0.7 to 0
- combining_map: bfloat16 [2048, 2048], P('tp', 'fs')
- valve_map: bfloat16 [2048, 3072], P('fs', 'tp'), may hold values from -0.125 to 0.125
- widening_map: bfloat16 [2048, 3072], P('fs', 'tp'), may hold values from -0.125 to 0.125
- valve_conv_stencil: bfloat16 [3, 3072], P(None, 'tp'), may hold values from -3.5 to 3.5
- widening_conv_stencil: bfloat16 [3, 3072], P(None, 'tp'), may hold values from -3.5 to 3.5
- narrowing_map: bfloat16 [3072, 2048], P('tp', 'fs')
Outputs:
- layer_out: bfloat16 [4096, 2048], P(('grp', 'fs'), 'tp'), parts along dimension 0
There are 2 independent parts, one for each index of `grp`. A program takes and returns all parts, laid end to end along the dimension named above; an argument that names none is the same for every part. Nothing has to cross between parts.
All inputs are finite; a program needn't handle non-finite values.
Results may differ from a plain program's by a relative error of at most 0.019.
Values may be sent and summed in bfloat16 or wider, within the bound.
A program may use at most 128 MiB of HBM per device.

v0:
```python
import functools

import jax
import jax.numpy as jnp
from jax import lax
from jax.experimental import pallas as pl
from jax.experimental.pallas import tpu as pltpu
from jax.sharding import PartitionSpec as P

KEY_DIM = 128
VALUE_DIM = 256
BLOCK = 16


epsilon = 1e-06
valve_steepness = 16.0
careful_evaluation = lax.Precision.HIGHEST


def norm_rows(values, channel_gain):
    return (
        values
        * lax.rsqrt(jnp.mean(values * values, axis=-1, keepdims=True) + epsilon)
        * channel_gain
    )


CHUNK = 64


def contract(left, right, left_dim, right_dim):
    return lax.dot_general(
        left.astype(jnp.bfloat16),
        right.astype(jnp.bfloat16),
        (((left_dim,), (right_dim,)), ((), ())),
        preferred_element_type=jnp.float32,
    )


def mixing_kernel(q_ref, k_ref, v_ref, low_ref, right_ref, valve_ref, excess_ref, gain_ref, out_ref):
    length = q_ref.shape[0]
    head_count = gain_ref.shape[0]
    rows = lax.broadcasted_iota(jnp.int32, (CHUNK, CHUNK), 0)
    columns = lax.broadcasted_iota(jnp.int32, (CHUNK, CHUNK), 1)
    lower = (columns <= rows).astype(jnp.float32)

    def one_chunk(index, states):
        span = pl.ds(pl.multiple_of(index * CHUNK, CHUNK), CHUNK)
        logits = (
            jnp.dot(
                low_ref[span, :],
                right_ref[...],
                precision=careful_evaluation,
                preferred_element_type=jnp.float32,
            )
            + valve_ref[...]
        )
        fading = (
            jnp.minimum(logits, 0.0) - jnp.log1p(jnp.exp(-jnp.abs(logits)))
        ) / valve_steepness + excess_ref[span, :]
        total = jnp.dot(
            lower, fading, precision=careful_evaluation, preferred_element_type=jnp.float32
        )
        after = []
        for head in range(head_count):
            key_span = slice(head * KEY_DIM, (head + 1) * KEY_DIM)
            value_span = slice(head * VALUE_DIM, (head + 1) * VALUE_DIM)
            cum = total[:, key_span]
            query = q_ref[span, key_span].astype(jnp.float32) * KEY_DIM ** (-0.5)
            key = k_ref[span, key_span].astype(jnp.float32)
            value = v_ref[span, value_span]
            state = states[head]
            pieces = []
            for block in range(CHUNK // BLOCK):
                low, high = block * BLOCK, (block + 1) * BLOCK
                start = cum[low - 1 : low] if block else jnp.zeros((1, KEY_DIM), jnp.float32)
                query_in = query[low:high] * jnp.exp(cum[low:high] - start)
                key_in = jnp.concatenate(
                    [key[:high] * jnp.exp(start - cum[:high])]
                    + ([jnp.zeros((CHUNK - high, KEY_DIM), jnp.float32)] if high < CHUNK else []),
                    axis=0,
                )
                pieces.append(contract(query_in, key_in, 1, 1))
            scores = jnp.where(columns <= rows, jnp.concatenate(pieces, axis=0), 0.0)
            tail = cum[CHUNK - 1 :]
            mixed = contract(scores, value, 1, 0) + contract(query * jnp.exp(cum), state, 1, 1)
            after.append(state * jnp.exp(tail) + contract(value, key * jnp.exp(tail - cum), 0, 0))
            out_ref[span, value_span] = norm_rows(mixed, gain_ref[head : head + 1, :]).astype(
                jnp.bfloat16
            )
        return tuple(after)

    empty = tuple(jnp.zeros((VALUE_DIM, KEY_DIM), jnp.float32) for _ in range(head_count))
    lax.fori_loop(0, length // CHUNK, one_chunk, empty, unroll=2)


def mixing(query, key, value, low, right, valve, excess, gain):
    length = query.shape[0]
    flops = length * value.shape[1] * 8 * KEY_DIM
    return pl.pallas_call(
        mixing_kernel,
        out_shape=jax.ShapeDtypeStruct(value.shape, jnp.bfloat16),
        in_specs=[pl.BlockSpec(memory_space=pltpu.VMEM)] * 8,
        out_specs=pl.BlockSpec(memory_space=pltpu.VMEM),
        cost_estimate=pl.CostEstimate(
            flops=60 * flops, bytes_accessed=8 * value.size, transcendentals=0
        ),
    )(query, key, value, low, right, valve, excess, gain)


def causal_taps(values, kernel):
    tap_count = kernel.shape[0]
    length = values.shape[0]
    padded = jnp.pad(values, ((tap_count - 1, 0), (0, 0)))
    kernel = kernel.astype(jnp.float32)
    summed = kernel[0] * padded[0:length]
    for offset in range(1, tap_count):
        summed = summed + kernel[offset] * padded[offset : offset + length]
    return summed


MESH = pl.DeviceIdType.MESH


def piece(ref, dimension, owner, part, full, cut, cuts):
    parts, line = lax.axis_size("grp"), lax.axis_size("fs")
    height = ref.shape[0] // (parts * cuts * (line if full and dimension == 0 else 1))
    first = part * cuts + cut
    if full and dimension == 0:
        first = owner * parts * cuts + first
    rows = pl.ds(pl.multiple_of(first * height, height), height)
    if not full or dimension == 0:
        return ref.at[rows, :]
    width = ref.shape[1] // line
    return ref.at[rows, pl.ds(pl.multiple_of(owner * width, width), width)]


def cuts_of(shard):
    parts = lax.axis_size("grp")
    cuts = 1
    while shard.size // (parts * 2 * cuts) >= 48 * 1024 and shard.shape[0] % (parts * 2 * cuts * 16) == 0:
        cuts *= 2
    return cuts


def gather_kernel(dimensions, cuts, spread, summed, *refs):
    count = len(dimensions)
    refs = list(refs)

    def take(number):
        taken = refs[:number]
        del refs[:number]
        return taken

    shards, block, partial = take(count), take(spread), take(summed)
    maps, rows_out = take(count), take(spread)
    total_out, squares_out = take(2) if summed else (None, None)
    if count:
        own_sem, line_send, line_recv, part_send, part_recv = take(5)
    if spread:
        spread_own, spread_send, spread_recv = take(3)
    if summed:
        pair_in, chip_sum, chip_in, squares_own, squares_in = take(5)
        pair_send, pair_recv, chip_send, chip_recv, squares_send, squares_recv = take(6)
    ranks, rank = lax.axis_size("tp"), lax.axis_index("tp")
    chips, chip, core = ranks // 2, rank // 2, lax.rem(rank, 2)

    def rank_at(offset):
        return lax.rem(rank + offset, ranks)

    def columns_of(ref, owner):
        width = ref.shape[1] // ranks
        return ref.at[:, pl.ds(pl.multiple_of(owner * width, width), width)]

    def spread_copy(offset, owner):
        return pltpu.make_async_remote_copy(
            src_ref=block[0],
            dst_ref=columns_of(rows_out[0], owner),
            send_sem=spread_send.at[offset],
            recv_sem=spread_recv.at[offset],
            device_id={"tp": rank_at(offset)},
            device_id_type=MESH,
        )

    def spread_local():
        return pltpu.make_async_copy(block[0], columns_of(rows_out[0], rank), spread_own)

    def pair_copy(target):
        return pltpu.make_async_remote_copy(
            src_ref=columns_of(partial[0], target * 2 + 1 - core),
            dst_ref=pair_in.at[target],
            send_sem=pair_send.at[target],
            recv_sem=pair_recv.at[target],
            device_id={"tp": chip * 2 + 1 - core},
            device_id_type=MESH,
        )

    def chip_copy(offset):
        return pltpu.make_async_remote_copy(
            src_ref=chip_sum.at[offset],
            dst_ref=chip_in.at[offset],
            send_sem=chip_send.at[offset],
            recv_sem=chip_recv.at[offset],
            device_id={"tp": lax.rem(chip + offset, chips) * 2 + core},
            device_id_type=MESH,
        )

    def squares_copy(offset):
        return pltpu.make_async_remote_copy(
            src_ref=squares_own,
            dst_ref=squares_in.at[offset],
            send_sem=squares_send.at[offset],
            recv_sem=squares_recv.at[offset],
            device_id={"tp": rank_at(offset)},
            device_id_type=MESH,
        )

    def sum_pairs():
        for target in range(chips):
            pair_copy(target).wait_recv()
        for offset in list(range(1, chips)) + [0]:
            target = lax.rem(chip + offset, chips)
            both = (
                columns_of(partial[0], target * 2 + core)[...].astype(jnp.float32)
                + pair_in[target].astype(jnp.float32)
            )
            if offset:
                chip_sum[offset] = both.astype(jnp.bfloat16)
                chip_copy(offset).start()
            else:
                total_out[...] = both

    def sum_chips():
        for offset in range(1, chips):
            chip_copy(offset).wait_recv()
            total_out[...] += chip_in[offset].astype(jnp.float32)
        total = total_out[...]
        squares_own[...] = lax.dot_general(
            jnp.ones((8, total.shape[1]), jnp.float32),
            total * total,
            (((1,), (1,)), ((), ())),
            precision=careful_evaluation,
            preferred_element_type=jnp.float32,
        )
        for offset in range(1, ranks):
            squares_copy(offset).start()
        summed_squares = squares_own[...]
        for offset in range(1, ranks):
            squares_copy(offset).wait_recv()
            summed_squares = summed_squares + squares_in[offset]
        squares_out[...] = lax.dot_general(
            summed_squares,
            jnp.full((8, 128), 0.125, jnp.float32),
            (((0,), (0,)), ((), ())),
            precision=careful_evaluation,
            preferred_element_type=jnp.float32,
        )
        for target in range(chips):
            pair_copy(target).wait_send()
        for offset in range(1, chips):
            chip_copy(offset).wait_send()
        for offset in range(1, ranks):
            squares_copy(offset).wait_send()

    pieces = [(which, cut) for which in range(count) for cut in range(cuts[which])]
    line, parts = lax.axis_size("fs"), lax.axis_size("grp")
    place, part = lax.axis_index("fs"), lax.axis_index("grp")

    def there(way):
        return place < line - 1 if way == 0 else place > 0

    def toward(way):
        return {"fs": place + 1 if way == 0 else place - 1}

    def part_of(offset):
        return lax.rem(part + offset, parts)

    def at(refs, unit, owner, half, full):
        which, cut = pieces[unit]
        return piece(refs[which], dimensions[which], owner, half, full, cut, cuts[which])

    def line_copy(unit, way, step):
        owner = place - step if way == 0 else place + step
        target = at(maps, unit, owner, part, True)
        return pltpu.make_async_remote_copy(
            src_ref=target,
            dst_ref=target,
            send_sem=line_send.at[unit, way, step],
            recv_sem=line_recv.at[unit, way, step],
            device_id=toward(way),
            device_id_type=MESH,
        )

    def first_copy(unit, way):
        return pltpu.make_async_remote_copy(
            src_ref=at(shards, unit, place, part, False),
            dst_ref=at(maps, unit, place, part, True),
            send_sem=line_send.at[unit, way, 0],
            recv_sem=line_recv.at[unit, way, 0],
            device_id=toward(way),
            device_id_type=MESH,
        )

    def arrival(unit, way, step):
        owner = place - step - 1 if way == 0 else place + step + 1
        target = at(maps, unit, owner, part, True)
        return pltpu.make_async_remote_copy(
            src_ref=target,
            dst_ref=target,
            send_sem=line_send.at[unit, way, step],
            recv_sem=line_recv.at[unit, way, step],
            device_id=toward(way),
            device_id_type=MESH,
        )

    def part_copy(unit, way, step, offset, coming):
        owner = place - step - 1 if way == 0 else place + step + 1
        mine = part_of(parts - offset) if coming else part
        target = at(maps, unit, owner, mine, True)
        return pltpu.make_async_remote_copy(
            src_ref=target,
            dst_ref=target,
            send_sem=part_send.at[unit, way, step, offset - 1],
            recv_sem=part_recv.at[unit, way, step, offset - 1],
            device_id={"grp": part_of(offset)},
            device_id_type=MESH,
        )

    def comes(way, step):
        return place - step - 1 >= 0 if way == 0 else place + step + 1 < line

    barrier = pltpu.get_barrier_semaphore()
    expected = 0
    if count:
        for way in range(2):

            @pl.when(there(way))
            def _():
                pl.semaphore_signal(barrier, inc=1, device_id=toward(way), device_id_type=MESH)

        for offset in range(1, parts):
            pl.semaphore_signal(
                barrier, inc=1, device_id={"grp": part_of(offset)}, device_id_type=MESH
            )
        expected = there(0).astype(jnp.int32) + there(1).astype(jnp.int32) + parts - 1
    if spread or summed:
        for offset in range(1, ranks):
            pl.semaphore_signal(
                barrier, inc=1, device_id={"tp": rank_at(offset)}, device_id_type=MESH
            )
        expected = expected + ranks - 1
    pl.semaphore_wait(barrier, expected)
    if summed:
        for target in range(chips):
            pair_copy(target).start()

    def begin(unit):
        for way in range(2):

            @pl.when(there(way))
            def _():
                first_copy(unit, way).start()

    def own_copy(which):
        height, width = shards[which].shape
        if dimensions[which] == 0:
            target = maps[which].at[pl.ds(pl.multiple_of(place * height, height), height), :]
        else:
            target = maps[which].at[:, pl.ds(pl.multiple_of(place * width, width), width)]
        return pltpu.make_async_copy(shards[which], target, own_sem.at[which])

    def pass_on(unit, step):
        for way in range(2):

            @pl.when(comes(way, step))
            def _():
                arrival(unit, way, step).wait_recv()

                @pl.when(there(way))
                def _():
                    line_copy(unit, way, step + 1).start()

                for offset in range(1, parts):
                    part_copy(unit, way, step, offset, False).start()

    if count:
        begin(0)
    if spread:
        for offset in range(1, ranks):
            spread_copy(offset, rank).start()
        spread_local().start()
    for which in range(count):
        own_copy(which).start()
    if summed:
        sum_pairs()
    for tick in range(len(pieces) + line - 2 if count else 0):
        if tick + 1 < len(pieces):
            begin(tick + 1)
        for step in range(line - 1):
            if 0 <= tick - step < len(pieces):
                pass_on(tick - step, step)

    if summed:
        sum_chips()
    if spread:
        spread_local().wait()
        for offset in range(1, ranks):
            spread_copy(offset, rank).wait_send()
            spread_copy(offset, rank_at(ranks - offset)).wait_recv()
    for which in range(count):
        own_copy(which).wait()
    for unit in range(len(pieces)):
        for way in range(2):

            @pl.when(there(way))
            def _():
                first_copy(unit, way).wait_send()

        @pl.loop(0, line - 1)
        def _(step):
            for way in range(2):

                @pl.when(comes(way, step))
                def _():
                    @pl.when(there(way))
                    def _():
                        line_copy(unit, way, step + 1).wait_send()

                    for offset in range(1, parts):
                        part_copy(unit, way, step, offset, False).wait_send()
                        part_copy(unit, way, step, offset, True).wait_recv()


def exchange(shards, dimensions, identity, block=None, partial=None):
    line, parts, ranks = lax.axis_size("fs"), lax.axis_size("grp"), lax.axis_size("tp")
    count = len(shards)
    cuts = [cuts_of(shard) for shard in shards]
    units = sum(cuts)
    spread, summed = int(block is not None), int(partial is not None)
    vmem, anywhere = pl.BlockSpec(memory_space=pltpu.VMEM), pl.BlockSpec(memory_space=pl.ANY)
    operands = list(shards)
    shapes = [
        jax.ShapeDtypeStruct(
            (shard.shape[0] * line, shard.shape[1])
            if dimension == 0
            else (shard.shape[0], shard.shape[1] * line),
            jnp.bfloat16,
        )
        for shard, dimension in zip(shards, dimensions)
    ]
    out_specs = [anywhere] * count
    scratch = []
    dma = pltpu.SemaphoreType.DMA
    if count:
        scratch += [dma((count,))] + [dma((units, 2, line))] * 2
        scratch += [dma((units, 2, line, max(parts - 1, 1)))] * 2
    if spread:
        operands.append(block)
        shapes.append(jax.ShapeDtypeStruct((block.shape[0], block.shape[1] * ranks), block.dtype))
        out_specs.append(anywhere)
        scratch += [dma] + [dma((ranks,))] * 2
    if summed:
        operands.append(partial)
        length, width = partial.shape[0], partial.shape[1] // ranks
        shapes += [
            jax.ShapeDtypeStruct((length, width), jnp.float32),
            jax.ShapeDtypeStruct((length, 128), jnp.float32),
        ]
        out_specs += [vmem] * 2
        scratch += [pltpu.VMEM((ranks // 2, length, width), jnp.bfloat16)] * 3
        scratch += [pltpu.VMEM((8, length), jnp.float32), pltpu.VMEM((ranks, 8, length), jnp.float32)]
        scratch += [dma((ranks // 2,))] * 4 + [dma((ranks,))] * 2
    return pl.pallas_call(
        functools.partial(gather_kernel, dimensions, cuts, spread, summed),
        out_shape=shapes,
        in_specs=[vmem] * len(operands),
        out_specs=out_specs,
        scratch_shapes=scratch,
        compiler_params=pltpu.CompilerParams(collective_id=identity, has_side_effects=True),
    )(*operands)


def on_device(
    block_source_tensor,
    attend_initial_norm_gain,
    each_channel_group_norm,
    attend_final_norm_gain,
    dense_initial_norm_gain,
    dense_final_norm_gain,
    question_map,
    address_map,
    payload_weights_map,
    fading_left_factor,
    fading_right_factor,
    fading_valve_constant,
    sudden_fade_excess,
    combining_map,
    valve_map,
    widening_map,
    valve_conv_stencil,
    widening_conv_stencil,
    narrowing_map,
):
    length, own_columns = block_source_tensor.shape
    tp_index = lax.axis_index("tp")
    full_width = own_columns * lax.axis_size("tp")
    question_full, address_full, payload_full, combining_full, full_rows = exchange(
        (question_map, address_map, payload_weights_map, combining_map),
        (0, 0, 0, 1),
        1,
        block=block_source_tensor,
    )
    normed = norm_rows(full_rows.astype(jnp.float32), attend_initial_norm_gain).astype(jnp.bfloat16)
    query, key, value = (
        jnp.dot(normed, full, preferred_element_type=jnp.float32).astype(jnp.bfloat16)
        for full in (question_full, address_full, payload_full)
    )
    low_rank = jnp.dot(normed, fading_left_factor, preferred_element_type=jnp.float32)
    head_out = mixing(
        query,
        key,
        value,
        low_rank,
        fading_right_factor,
        fading_valve_constant[None],
        sudden_fade_excess,
        each_channel_group_norm,
    )
    partials = jnp.dot(
        head_out,
        combining_full,
        preferred_element_type=jnp.float32,
    )
    valve_full, mixed, squares = exchange(
        (valve_map,), (0,), 2, partial=partials.astype(jnp.bfloat16)
    )
    own_gain = lax.dynamic_slice_in_dim(attend_final_norm_gain, tp_index * own_columns, own_columns)
    first = (
        block_source_tensor.astype(jnp.float32)
        + mixed * lax.rsqrt(squares[:, :1] / full_width + epsilon) * own_gain
    ).astype(jnp.bfloat16)
    widening_full, narrowing_full, first_rows = exchange(
        (widening_map, narrowing_map), (0, 1), 3, block=first
    )
    ffn_in = norm_rows(first_rows.astype(jnp.float32), dense_initial_norm_gain).astype(jnp.bfloat16)

    gate_pre = jnp.dot(ffn_in, valve_full, preferred_element_type=jnp.float32)
    up_pre = jnp.dot(ffn_in, widening_full, preferred_element_type=jnp.float32)
    hidden = (
        jax.nn.silu(causal_taps(gate_pre, valve_conv_stencil))
        * causal_taps(up_pre, widening_conv_stencil)
    ).astype(jnp.bfloat16)
    down_partials = jnp.dot(
        hidden,
        narrowing_full,
        preferred_element_type=jnp.float32,
    )
    channel, channel_squares = exchange((), (), 4, partial=down_partials.astype(jnp.bfloat16))
    own_post = lax.dynamic_slice_in_dim(dense_final_norm_gain, tp_index * own_columns, own_columns)
    return (
        first.astype(jnp.float32)
        + channel * lax.rsqrt(channel_squares[:, :1] / full_width + epsilon) * own_post
    ).astype(jnp.bfloat16)


def solution(mesh):
    placed = (
        P(("grp", "fs"), "tp"),
        P(),
        P("tp", None),
        P(),
        P(),
        P(),
        P("fs", "tp"),
        P("fs", "tp"),
        P("fs", "tp"),
        P(),
        P(None, "tp"),
        P("tp"),
        P(("grp", "fs"), "tp"),
        P("tp", "fs"),
        P("fs", "tp"),
        P("fs", "tp"),
        P(None, "tp"),
        P(None, "tp"),
        P("tp", "fs"),
    )
    return jax.shard_map(
        on_device, mesh=mesh, in_specs=placed, out_specs=P(("grp", "fs"), "tp"), check_vma=False
    )
```

profile of v0, /device:TPU:0, one launch (start us, length us, event | category | flops | bytes accessed | tf_op | source)
XLA Modules:
  0.0 232.0 jit_solution(18289686334379813703)
XLA Ops:
  0.0 0.0 copy-start
  0.0 0.0 copy-start.12
  0.0 65.3 %shard_map.181 = (bf16[2048,256]{1,0:T(8,128)(2,1)}, bf16[2048,256]{1,0:T(8,128)(2,1)}, bf16[2048,512]{1,0:T(8,128)(2,1)}, bf16[512,2048]{1,0:T(8,128)(2,1)}, bf16[512,2048]{1,0:T(8,128)(2,1)}) custom-call(bf16[512,256]{1,0:T(8,128)(2,1)} %refs_0_.3, bf16[512,256]{1,0:T(8,128)(2,1)} %refs_1_.2, bf16[512,512]{1,0:T(8,128)(2,1)} %refs_2_.1, ...), custom_call_target="tpu_custom_call" | custom-call | tf_op jit(solution)/shard_map/pallas_call | solution.py:473
  65.3 0.0 copy-start.2
  65.3 2.2 fusion
  67.6 0.0 copy-done.12
  67.6 0.0 copy-done.2
  67.6 0.0 copy-start.11
  67.6 3.8 %convolution_convert_fusion.2.v_ref = bf16[512,512]{1,0:T(8,128)(2,1)} fusion(bf16[2048,512]{1,0:T(8,128)(2,1)} %get-tuple-element.21, bf16[512,2048]{1,0:T(8,128)(2,1)S(1)} %copy-done.2, f32[2048]{0:T(1024)S(1)} %copy-done.12, f32[512]{0:T(512)S(1)} %add_rsqrt_fusion.1), kind=kOutput, calls=%fused_computation.13 | convolution fusion | flops 1078198272 | bytes 4728832 | tf_op jit(solution)/shard_map/dot_general | solution.py:515
  71.4 0.0 copy-done.11
  71.4 0.0 copy-start.10
  71.4 1.5 convolution_convert_fusion.3.k_ref
  72.8 0.0 copy-done.10
  72.9 1.5 convolution_convert_fusion.4.q_ref
  74.3 0.0 copy-done
  74.3 1.5 fusion.19.low_ref
  75.8 0.0 copy-start.9
  75.8 8.9 %shard_map.182 = bf16[512,512]{1,0:T(8,128)(2,1)} custom-call(bf16[512,256]{1,0:T(8,128)(2,1)} %convolution_convert_fusion.4.q_ref, bf16[512,256]{1,0:T(8,128)(2,1)} %convolution_convert_fusion.3.k_ref, bf16[512,512]{1,0:T(8,128)(2,1)} %convolution_convert_fusion.2.v_ref, f32[512,16]{1,0:T(8,128)} %fusion.19.low_ref, f32[16,256]{1,0:T(8,128)} %right_ref.1, ...), custom_call_target="tpu_custom_call" | custom-call | flops 16106127360 | bytes 2097152 | tf_op jit(solution)/shard_map/pallas_call | solution.py:100
  84.7 0.0 copy-done.9
  84.7 3.7 %convolution_convert_fusion.1.refs_1_ = bf16[512,2048]{1,0:T(8,128)(2,1)} fusion(bf16[512,512]{1,0:T(8,128)(2,1)} %shard_map.182, bf16[512,2048]{1,0:T(8,128)(2,1)S(1)} %copy-done.9), kind=kOutput, calls=%fused_computation.11 | convolution fusion | flops 1074790400 | bytes 4718592 | tf_op jit(solution)/shard_map/dot_general | solution.py:529
  88.4 0.0 copy-start.4
  88.4 37.2 %shard_map.183 = (bf16[2048,768]{1,0:T(8,128)(2,1)}, f32[512,512]{1,0:T(8,128)}, f32[512,128]{1,0:T(8,128)}) custom-call(bf16[512,768]{1,0:T(8,128)(2,1)} %refs_0_.4, bf16[512,2048]{1,0:T(8,128)(2,1)} %convolution_convert_fusion.1.refs_1_), custom_call_target="tpu_custom_call" | custom-call | tf_op jit(solution)/shard_map/pallas_call | solution.py:473
  125.5 1.1 rsqrt_reduce_fusion.1
  126.7 0.8 dynamic_slice.6
  127.4 0.0 copy-done.4
  127.4 2.2 add_convert_fusion.1.refs_2_
  129.7 0.0 copy-start.13
  129.7 61.8 %shard_map.184 = (bf16[2048,768]{1,0:T(8,128)(2,1)}, bf16[768,2048]{1,0:T(8,128)(2,1)}, bf16[512,2048]{1,0:T(8,128)(2,1)}) custom-call(bf16[512,768]{1,0:T(8,128)(2,1)} %refs_0_.5, bf16[768,512]{1,0:T(8,128)(2,1)} %refs_1_.3, bf16[512,512]{1,0:T(8,128)(2,1)} %add_convert_fusion.1.refs_2_), custom_call_target="tpu_custom_call" | custom-call | tf_op jit(solution)/shard_map/pallas_call | solution.py:473
  191.5 0.0 copy-start.3
  191.5 2.2 fusion.3
  193.7 0.0 copy-done.13
  193.7 0.0 copy-done.3
  193.7 0.0 copy-start.8
  193.7 3.9 %fusion.15 = f32[512,768]{1,0:T(8,128)S(1)} fusion(bf16[2048,768]{1,0:T(8,128)(2,1)} %get-tuple-element.26, bf16[512,2048]{1,0:T(8,128)(2,1)S(1)} %copy-done.3, f32[2048]{0:T(1024)S(1)} %copy-done.13, f32[512]{0:T(512)S(1)} %add_rsqrt_fusion), kind=kOutput, calls=%fused_computation.26 | convolution fusion | flops 1614807040 | bytes 6825984 | tf_op jit(solution)/shard_map/dot_general | solution.py:547
  197.7 0.0 copy-done.8
  197.7 0.0 copy-start.5
  197.7 0.0 copy-start.6
  197.7 0.0 copy-start.7
  197.7 1.9 fusion.13
  199.6 0.0 copy-done.5
  199.6 0.0 copy-done.6
  199.6 0.1 slice_reduce_fusion.2
  199.7 0.0 copy-done.7
  199.7 4.1 %convolution_convert_fusion.refs_0_ = bf16[512,2048]{1,0:T(8,128)(2,1)} fusion(bf16[768,2048]{1,0:T(8,128)(2,1)S(1)} %copy-done.7, f32[512,768]{1,0:T(8,128)S(1)} %fusion.13, f32[512,768]{1,0:T(8,128)S(1)} %fusion.15, f32[768]{0:T(1024)S(1)} %get-tuple-element.35, f32[768]{0:T(1024)S(1)} %get-tuple-element.36, f32[768]{0:T(1024)S(1)} %get-tuple-element.34, ...), kind=kOutput, calls=%fused_computation.10 | convolution fusion | flops 1617952768 | bytes 8407040 | tf_op jit(solution)/shard_map/dot_general | solution.py:553
  203.8 0.0 copy-start.1
  203.8 24.1 %shard_map.185 = (f32[512,512]{1,0:T(8,128)}, f32[512,128]{1,0:T(8,128)}) custom-call(bf16[512,2048]{1,0:T(8,128)(2,1)} %convolution_convert_fusion.refs_0_), custom_call_target="tpu_custom_call" | custom-call | tf_op jit(solution)/shard_map/pallas_call | solution.py:473
  227.9 1.1 rsqrt_reduce_fusion
  229.0 0.8 dynamic_slice.7
  229.7 0.0 copy-done.1
  229.8 2.2 add_convert_fusion
  (4 shorter events, 0.0 us)
Async XLA Ops:
  0.0 74.3 %copy-start = (bf16[2048,16]{0,1:T(8,128)(2,1)S(1)}, bf16[2048,16]{0,1:T(8,128)(2,1)}, u32[]{:S(2)}) copy-start(bf16[2048,16]{0,1:T(8,128)(2,1)} %param.28) | copy-start | bytes 196612
  0.0 67.6 %copy-start.12 = (f32[2048]{0:T(1024)S(1)}, f32[2048]{0:T(1024)}, u32[]{:S(2)}) copy-start(f32[2048]{0:T(1024)} %param.20) | copy-start | bytes 24580
  65.3 2.3 copy-start.2
  67.6 3.8 %copy-start.11 = (bf16[2048,256]{1,0:T(8,128)(2,1)S(1)}, bf16[2048,256]{1,0:T(8,128)(2,1)}, u32[]{:S(2)}) copy-start(bf16[2048,256]{1,0:T(8,128)(2,1)} %get-tuple-element.20) | copy-start | bytes 3145732
  71.4 1.5 copy-start.10
  75.8 8.9 %copy-start.9 = (bf16[512,2048]{1,0:T(8,128)(2,1)S(1)}, bf16[512,2048]{1,0:T(8,128)(2,1)}, u32[]{:S(2)}) copy-start(bf16[512,2048]{1,0:T(8,128)(2,1)} %get-tuple-element.22) | copy-start | bytes 6291460
  88.4 39.0 %copy-start.4 = (bf16[512,512]{1,0:T(8,128)(2,1)S(1)}, bf16[512,512]{1,0:T(8,128)(2,1)}, u32[]{:S(2)}) copy-start(bf16[512,512]{1,0:T(8,128)(2,1)} %refs_4_.1) | copy-start | bytes 1572868
  129.7 64.1 %copy-start.13 = (f32[2048]{0:T(1024)S(1)}, f32[2048]{0:T(1024)}, u32[]{:S(2)}) copy-start(f32[2048]{0:T(1024)} %param.23) | copy-start | bytes 24580
  191.5 2.3 copy-start.3
  193.7 3.9 %copy-start.8 = (bf16[2048,768]{1,0:T(8,128)(2,1)S(1)}, bf16[2048,768]{1,0:T(8,128)(2,1)}, u32[]{:S(2)}) copy-start(bf16[2048,768]{1,0:T(8,128)(2,1)} %get-tuple-element.27) | copy-start | bytes 9437188
  197.7 1.9 copy-start.5
  197.7 1.9 copy-start.6
  197.7 2.0 copy-start.7
  203.8 26.0 %copy-start.1 = (bf16[512,512]{1,0:T(8,128)(2,1)S(1)}, bf16[512,512]{1,0:T(8,128)(2,1)}, u32[]{:S(2)}) copy-start(bf16[512,512]{1,0:T(8,128)(2,1)} %add_convert_fusion.1.refs_2_) | copy-start | bytes 1572868
where the time goes:
time: 232 us
  Pallas kernels  197 us (85%)
  matrix products  21.8 us (9%)
  other arithmetic  11.2 us (5%)
    pallas_call x4, Pallas kernels, exchange(): pl.pallas_call(functools.partial(gather_kernel, dimensions, cuts, spread,...  188 us
    pallas_call x1, Pallas kernels, mixing(): pl.pallas_call(mixing_kernel, out_shape=jax.ShapeDtypeStruct(value.shape,...  8.86 us
    dot_general x3, matrix products, on_device(): jnp.dot(normed, full, preferred_element_type=jnp.float32)  6.75 us

commit v1 on v0

v1 whole, which is shorter than its diff:
```python
import functools

import jax
import jax.numpy as jnp
from jax import lax
from jax.experimental import pallas as pl
from jax.experimental.pallas import tpu as pltpu
from jax.sharding import PartitionSpec as P

KEY_DIM = 128
VALUE_DIM = 256
BLOCK = 16
CHUNK = 64

epsilon = 1e-06
valve_steepness = 16.0
careful_evaluation = lax.Precision.HIGHEST

MESH = pl.DeviceIdType.MESH
f32, bf16 = jnp.float32, jnp.bfloat16

AHEAD = 2
STEP_BUDGET = 4.5


def norm_rows(values, channel_gain):
    return (
        values
        * lax.rsqrt(jnp.mean(values * values, axis=-1, keepdims=True) + epsilon)
        * channel_gain
    )


def tile_of(width):
    return 256 if width % 256 == 0 else 128


def halves(values):
    high = values.astype(bf16)
    return high, (values - high.astype(f32)).astype(bf16)


def contract(left, right, left_dim, right_dim):
    return lax.dot_general(
        left, right, (((left_dim,), (right_dim,)), ((), ())), preferred_element_type=f32
    )


def contract_careful(left, right):
    left_high, left_low = halves(left)
    right_high, right_low = halves(right)
    return contract(
        jnp.concatenate([left_high, left_high, left_low], axis=1),
        jnp.concatenate([right_high, right_low, right_high], axis=1),
        1,
        1,
    )


def cuts_of(shard, parts):
    cuts = 1
    while shard.size // (parts * 2 * cuts) >= 48 * 1024 and shard.shape[0] % (parts * 2 * cuts * 16) == 0:
        cuts *= 2
    return cuts


def layer_kernel(config, *refs):
    cuts, down_cuts, line, parts, ranks = config
    refs = list(refs)

    def take(number):
        taken = refs[:number]
        del refs[:number]
        return taken

    block, first_gain, head_gain, mixed_gain, second_gain, last_gain = take(6)
    left, right, valve, excess, gate_taps, up_taps = take(6)
    shards = take(7)
    (out,) = take(1)
    maps = take(7)
    rows_full, first_full, normed, query, key, value, low, head_out, states = take(9)
    partial, pair_in, chip_sum, chip_in, total, squares_own, squares_in, first = take(8)
    padded, gate_act, hidden, down_partial, down_pair, down_sum, down_in, down_total = take(8)
    down_squares_own, down_squares_in = take(2)
    own_sem, line_send, line_recv, part_send, part_recv = take(5)
    spread_own, spread_send, spread_recv = take(3)
    pair_send, pair_recv, chip_send, chip_recv, squares_send, squares_recv = take(6)

    length, own = block.shape
    width = own * ranks
    chips = ranks // 2
    rank = lax.axis_index("tp")
    chip, core = rank // 2, lax.rem(rank, 2)
    place, part = lax.axis_index("fs"), lax.axis_index("grp")
    head_count = head_gain.shape[0]
    own_columns = pl.ds(pl.multiple_of(rank * own, own), own)

    def rank_at(offset):
        return lax.rem(rank + offset, ranks)

    units = []
    for which in range(7):
        for cut in range(cuts[which]):
            units.append((which, cut))
    unit_count = len(units)
    first_unit = [sum(cuts[:which]) for which in range(8)]

    def there(way):
        return place < line - 1 if way == 0 else place > 0

    def toward(way):
        return {"fs": place + 1 if way == 0 else place - 1}

    def comes(way, step):
        return place - step - 1 >= 0 if way == 0 else place + step + 1 < line

    def part_of(offset):
        return lax.rem(part + offset, parts)

    def at(full, unit, owner, half):
        which, cut = units[unit]
        ref = maps[which] if full else shards[which]
        shard_rows, shard_columns = shards[which].shape
        if which == 6:
            height, wide = shard_rows // parts, shard_columns // cuts[which]
            row, column = half * height, cut * wide
            if full:
                column = owner * shard_columns + cut * wide
        else:
            height, wide = shard_rows // (parts * cuts[which]), shard_columns
            row, column = (half * cuts[which] + cut) * height, 0
            if full and which == 3:
                column = owner * shard_columns
            elif full:
                row = owner * shard_rows + row
        rows = pl.ds(pl.multiple_of(row, height), height)
        if wide == ref.shape[1]:
            return ref.at[rows, :]
        return ref.at[rows, pl.ds(pl.multiple_of(column, wide), wide)]

    def remote(source, target, send, recv, device):
        return pltpu.make_async_remote_copy(
            src_ref=source,
            dst_ref=target,
            send_sem=send,
            recv_sem=recv,
            device_id=device,
            device_id_type=MESH,
        )

    def first_copy(unit, way):
        return remote(
            at(False, unit, place, part),
            at(True, unit, place, part),
            line_send.at[unit, way, 0],
            line_recv.at[unit, way, 0],
            toward(way),
        )

    def line_copy(unit, way, step):
        target = at(True, unit, place - step if way == 0 else place + step, part)
        return remote(
            target, target, line_send.at[unit, way, step], line_recv.at[unit, way, step], toward(way)
        )

    def arrival(unit, way, step):
        target = at(True, unit, place - step - 1 if way == 0 else place + step + 1, part)
        return remote(
            target, target, line_send.at[unit, way, step], line_recv.at[unit, way, step], toward(way)
        )

    def part_copy(unit, way, step, offset, coming):
        mine = part_of(parts - offset) if coming else part
        target = at(True, unit, place - step - 1 if way == 0 else place + step + 1, mine)
        return remote(
            target,
            target,
            part_send.at[unit, way, step, offset - 1],
            part_recv.at[unit, way, step, offset - 1],
            {"grp": part_of(offset)},
        )

    def own_copy(which):
        height, wide = shards[which].shape
        if which in (3, 6):
            target = maps[which].at[:, pl.ds(pl.multiple_of(place * wide, wide), wide)]
        else:
            target = maps[which].at[pl.ds(pl.multiple_of(place * height, height), height), :]
        return pltpu.make_async_copy(shards[which], target, own_sem.at[which])

    def begin(unit):
        for way in range(2):

            @pl.when(there(way))
            def _():
                first_copy(unit, way).start()

    def pass_on(unit, step):
        for way in range(2):

            @pl.when(comes(way, step))
            def _():
                arrival(unit, way, step).wait_recv()

                if step < line - 2:

                    @pl.when(there(way))
                    def _():
                        line_copy(unit, way, step + 1).start()

                for offset in range(1, parts):
                    part_copy(unit, way, step, offset, False).start()

    def finish(unit):
        @pl.loop(0, line - 1)
        def _(step):
            for way in range(2):

                @pl.when(comes(way, step))
                def _():
                    for offset in range(1, parts):
                        part_copy(unit, way, step, offset, True).wait_recv()

    def drain(unit):
        for way in range(2):

            @pl.when(there(way))
            def _():
                first_copy(unit, way).wait_send()

        @pl.loop(0, line - 1)
        def _(step):
            for way in range(2):

                @pl.when(comes(way, step))
                def _():
                    @pl.when(there(way))
                    def _():
                        line_copy(unit, way, step + 1).wait_send()

                    for offset in range(1, parts):
                        part_copy(unit, way, step, offset, False).wait_send()

    def columns_of(ref, owner):
        return ref.at[:, pl.ds(pl.multiple_of(owner * own, own), own)]

    def spread_copy(turn, source, full, offset, owner):
        return remote(
            source,
            columns_of(full, owner),
            spread_send.at[turn, offset],
            spread_recv.at[turn, offset],
            {"tp": rank_at(offset)},
        )

    def spread_local(turn, source, full):
        return pltpu.make_async_copy(source, columns_of(full, rank), spread_own.at[turn])

    def spread_start(turn, source, full):
        for offset in range(1, ranks):
            spread_copy(turn, source, full, offset, rank).start()
        spread_local(turn, source, full).start()

    def spread_wait(turn, source, full):
        spread_local(turn, source, full).wait()
        for offset in range(1, ranks):
            spread_copy(turn, source, full, offset, rank_at(ranks - offset)).wait_recv()

    def spread_drain(turn, source, full):
        for offset in range(1, ranks):
            spread_copy(turn, source, full, offset, rank).wait_send()

    def sum_refs(turn):
        if turn == 0:
            return partial, pair_in, chip_sum, chip_in, total
        unit = turn - 1
        wide = own // down_cuts
        return (
            down_partial.at[unit],
            down_pair.at[unit],
            down_sum.at[unit],
            down_in.at[unit],
            down_total.at[:, pl.ds(unit * wide, wide)],
        )

    def pair_copy(turn, target):
        source, landing = sum_refs(turn)[:2]
        return remote(
            source.at[target * 2 + 1 - core],
            landing.at[target],
            pair_send.at[turn, target],
            pair_recv.at[turn, target],
            {"tp": chip * 2 + 1 - core},
        )

    def chip_copy(turn, offset):
        _, _, source, landing, _ = sum_refs(turn)
        return remote(
            source.at[offset],
            landing.at[offset],
            chip_send.at[turn, offset],
            chip_recv.at[turn, offset],
            {"tp": lax.rem(chip + offset, chips) * 2 + core},
        )

    def sum_pairs(turn):
        source, landing, sums, _, result = sum_refs(turn)
        for target in range(chips):
            pair_copy(turn, target).wait_recv()
        for offset in list(range(1, chips)) + [0]:
            target = lax.rem(chip + offset, chips)
            both = source[target * 2 + core].astype(f32) + landing[target].astype(f32)
            if offset:
                sums[offset] = both.astype(bf16)
                chip_copy(turn, offset).start()
            else:
                result[...] = both

    def sum_chips(turn):
        _, _, _, landing, result = sum_refs(turn)
        for offset in range(1, chips):
            chip_copy(turn, offset).wait_recv()
            result[...] += landing[offset].astype(f32)

    def sums_drain(turn):
        for target in range(chips):
            pair_copy(turn, target).wait_send()
        for offset in range(1, chips):
            chip_copy(turn, offset).wait_send()

    def squares_copy(turn, offset):
        source, landing = ((squares_own, squares_in), (down_squares_own, down_squares_in))[turn]
        return remote(
            source,
            landing.at[offset],
            squares_send.at[turn, offset],
            squares_recv.at[turn, offset],
            {"tp": rank_at(offset)},
        )

    def squares_start(turn, values_ref):
        values = values_ref[...]
        (squares_own, down_squares_own)[turn][...] = lax.dot_general(
            jnp.ones((8, own), f32),
            values * values,
            (((1,), (1,)), ((), ())),
            precision=careful_evaluation,
            preferred_element_type=f32,
        )
        for offset in range(1, ranks):
            squares_copy(turn, offset).start()

    def squares_wait(turn):
        source, landing = ((squares_own, squares_in), (down_squares_own, down_squares_in))[turn]
        summed = source[...]
        for offset in range(1, ranks):
            squares_copy(turn, offset).wait_recv()
            summed = summed + landing[offset]
        columns = lax.dot_general(
            summed,
            jnp.full((8, 128), 0.125, f32),
            (((0,), (0,)), ((), ())),
            precision=careful_evaluation,
            preferred_element_type=f32,
        )
        return lax.rsqrt(columns[:, :1] / width + epsilon)

    def norm_into(source, gain):
        tall = 64

        def one(index, carry):
            rows = pl.ds(pl.multiple_of(index * tall, tall), tall)
            normed[rows, :] = norm_rows(source[rows, :].astype(f32), gain[...]).astype(bf16)
            return carry

        lax.fori_loop(0, length // tall, one, 0)

    def over_columns(ref_width, body):
        wide = tile_of(ref_width)

        def one(index, carry):
            body(pl.ds(pl.multiple_of(index * wide, wide), wide))
            return carry

        lax.fori_loop(0, ref_width // wide, one, 0)

    def project(which, target):
        def body(columns):
            target[:, columns] = jnp.dot(
                normed[...], maps[which][:, columns], preferred_element_type=f32
            ).astype(bf16)

        over_columns(maps[which].shape[1], body)

    def low_rank():
        low[...] = jnp.dot(normed[...], left[...], preferred_element_type=f32)

    def one_chunk(index, carried):
        rows = lax.broadcasted_iota(jnp.int32, (CHUNK, CHUNK), 0)
        columns = lax.broadcasted_iota(jnp.int32, (CHUNK, CHUNK), 1)
        lower = (columns <= rows).astype(f32)
        span = pl.ds(pl.multiple_of(index * CHUNK, CHUNK), CHUNK)
        logits = (
            jnp.dot(
                low[span, :],
                right[...],
                precision=careful_evaluation,
                preferred_element_type=f32,
            )
            + valve[...]
        )
        fading = (
            jnp.minimum(logits, 0.0) - jnp.log1p(jnp.exp(-jnp.abs(logits)))
        ) / valve_steepness + excess[span, :]
        summed = jnp.dot(
            lower, fading, precision=careful_evaluation, preferred_element_type=f32
        )
        after = []
        for head in range(head_count):
            key_span = slice(head * KEY_DIM, (head + 1) * KEY_DIM)
            value_span = slice(head * VALUE_DIM, (head + 1) * VALUE_DIM)
            cum = summed[:, key_span]
            queries = query[span, key_span].astype(f32) * KEY_DIM ** (-0.5)
            keys = key[span, key_span].astype(f32)
            values = value[span, value_span]
            state = carried[head]
            pieces = []
            for piece in range(CHUNK // BLOCK):
                bottom, top = piece * BLOCK, (piece + 1) * BLOCK
                start = cum[bottom - 1 : bottom] if piece else jnp.zeros((1, KEY_DIM), f32)
                query_in = queries[bottom:top] * jnp.exp(cum[bottom:top] - start)
                key_in = jnp.concatenate(
                    [keys[:top] * jnp.exp(start - cum[:top])]
                    + ([jnp.zeros((CHUNK - top, KEY_DIM), f32)] if top < CHUNK else []),
                    axis=0,
                )
                pieces.append(contract_careful(query_in, key_in))
            scores = jnp.where(columns <= rows, jnp.concatenate(pieces, axis=0), 0.0)
            tail = cum[CHUNK - 1 :]
            score_high, score_low = halves(scores)
            mixed = (
                contract(score_high, values, 1, 0)
                + contract(score_low, values, 1, 0)
                + contract_careful(queries * jnp.exp(cum), state)
            )
            end_high, end_low = halves(keys * jnp.exp(tail - cum))
            after.append(
                state * jnp.exp(tail)
                + contract(
                    jnp.concatenate([values, values], axis=0),
                    jnp.concatenate([end_high, end_low], axis=0),
                    0,
                    0,
                )
            )
            head_out[span, value_span] = norm_rows(mixed, head_gain[head : head + 1, :]).astype(bf16)
        return tuple(after)

    chunk_count = length // CHUNK
    chunk_step = max(1, chunk_count // 4)

    def mix(start):
        if start == 0:
            carried = tuple(jnp.zeros((VALUE_DIM, KEY_DIM), f32) for _ in range(head_count))
        else:
            carried = tuple(states[head] for head in range(head_count))
        carried = lax.fori_loop(start, min(start + chunk_step, chunk_count), one_chunk, carried)
        for head in range(head_count):
            states[head] = carried[head]

    def combine():
        for target in range(ranks):

            def body(columns, target=target):
                columns_full = pl.ds(
                    pl.multiple_of(target * own + columns.start, columns.size), columns.size
                )
                partial[target, :, columns] = jnp.dot(
                    head_out[...], maps[3][:, columns_full], preferred_element_type=f32
                ).astype(bf16)

            over_columns(own, body)

    def start_pairs(turn):
        for target in range(chips):
            pair_copy(turn, target).start()

    def make_first():
        scale = squares_wait(0)
        first[...] = (
            block[...].astype(f32) + total[...] * scale * mixed_gain[:, own_columns]
        ).astype(bf16)
        spread_start(1, first, first_full)

    def taps(kernel_ref, columns):
        kernel_rows = kernel_ref[:, columns].astype(f32)
        tap_count = kernel_ref.shape[0]
        summed = None
        for tap in range(tap_count):
            shift = padded_rows - (tap_count - 1) + tap
            term = kernel_rows[tap : tap + 1] * padded[shift : shift + length, :]
            summed = term if summed is None else summed + term
        return summed

    padded_rows = padded.shape[0] - length

    def gate():
        padded[0:padded_rows, :] = jnp.zeros((padded_rows, padded.shape[1]), f32)

        def body(columns):
            padded[padded_rows:, :] = jnp.dot(
                normed[...], maps[4][:, columns], preferred_element_type=f32
            )
            turned = taps(gate_taps, columns)
            gate_act[:, columns] = turned / (1.0 + jnp.exp(-turned))

        over_columns(maps[4].shape[1], body)

    def up():
        def body(columns):
            padded[padded_rows:, :] = jnp.dot(
                normed[...], maps[5][:, columns], preferred_element_type=f32
            )
            hidden[:, columns] = (gate_act[:, columns] * taps(up_taps, columns)).astype(bf16)

        over_columns(maps[5].shape[1], body)

    def down(unit):
        wide = own // down_cuts

        def one(target, carry):
            columns = pl.ds(pl.multiple_of(target * own + unit * wide, wide), wide)
            down_partial[unit, target] = jnp.dot(
                hidden[...], maps[6][:, columns], preferred_element_type=f32
            ).astype(bf16)
            return carry

        lax.fori_loop(0, ranks, one, 0)
        start_pairs(1 + unit)

    def last():
        scale = squares_wait(1)
        out[...] = (
            first[...].astype(f32) + down_total[...] * scale * last_gain[:, own_columns]
        ).astype(bf16)

    barrier = pltpu.get_barrier_semaphore()
    for way in range(2):

        @pl.when(there(way))
        def _():
            pl.semaphore_signal(barrier, inc=1, device_id=toward(way), device_id_type=MESH)

    for offset in range(1, parts):
        pl.semaphore_signal(barrier, inc=1, device_id={"grp": part_of(offset)}, device_id_type=MESH)
    for offset in range(1, ranks):
        pl.semaphore_signal(barrier, inc=1, device_id={"tp": rank_at(offset)}, device_id_type=MESH)
    pl.semaphore_wait(
        barrier, there(0).astype(jnp.int32) + there(1).astype(jnp.int32) + parts - 1 + ranks - 1
    )

    for unit in range(min(AHEAD, unit_count)):
        begin(unit)
    spread_start(0, block, rows_full)
    for which in range(7):
        own_copy(which).start()

    jobs = []
    landed = [0]
    loaded = set()

    def job(needs, gap, cost, *work):
        jobs.append((needs, gap, cost, work))

    def whole(which):
        return first_unit[which + 1] - 1

    job(-1, 2, 3.0, lambda: spread_wait(0, block, rows_full), lambda: norm_into(rows_full, first_gain), low_rank)
    job(whole(0), 0, 1.5, lambda: project(0, query))
    job(whole(1), 0, 1.5, lambda: project(1, key))
    job(whole(2), 0, 3.5, lambda: project(2, value))
    for start in range(0, chunk_count, chunk_step):
        job(whole(2), 0, 3.0, functools.partial(mix, start))
    job(whole(3), 0, 4.0, combine, lambda: start_pairs(0))
    job(-1, 1, 2.0, lambda: sum_pairs(0))
    job(-1, 2, 2.0, lambda: sum_chips(0), lambda: squares_start(0, total))
    job(-1, 1, 2.0, make_first)
    job(-1, 3, 2.5, lambda: spread_wait(1, first, first_full), lambda: norm_into(first_full, second_gain))
    job(whole(4), 0, 4.5, gate)
    job(whole(5), 0, 4.5, up)
    for unit in range(down_cuts):
        job(first_unit[6] + unit, 0, 1.0, functools.partial(down, unit))
        if unit:
            job(-1, 0, 1.0, functools.partial(sum_pairs, unit))
    job(-1, 0, 1.0, functools.partial(sum_pairs, down_cuts))
    for unit in range(down_cuts):
        job(-1, 0, 0.5, functools.partial(sum_chips, 1 + unit))
    job(-1, 0, 1.0, lambda: squares_start(1, down_total))
    job(-1, 0, 1.0, last)

    def land(needs):
        while landed[0] <= needs:
            unit = landed[0]
            which = units[unit][0]
            if which not in loaded:
                loaded.add(which)
                own_copy(which).wait()
            finish(unit)
            landed[0] += 1

    at_step = -1
    spent = 0.0
    previous = 0
    for tick in range(unit_count + line - 2):
        if tick + AHEAD < unit_count:
            begin(tick + AHEAD)
        for step in range(line - 1):
            if 0 <= tick - step < unit_count:
                pass_on(tick - step, step)
        spent = 0.0
        while jobs:
            needs, gap, cost, work = jobs[0]
            if spent + cost > STEP_BUDGET and spent > 0.0:
                break
            if tick < needs + line - 1 or tick < previous + gap:
                break
            jobs.pop(0)
            land(needs)
            for act in work:
                act()
            spent += cost
            previous = tick
    for needs, _, _, work in jobs:
        land(needs)
        for act in work:
            act()

    for unit in range(unit_count):
        drain(unit)
    spread_drain(0, block, rows_full)
    spread_drain(1, first, first_full)
    for turn in range(1 + down_cuts):
        sums_drain(turn)
    for turn in range(2):
        for offset in range(1, ranks):
            squares_copy(turn, offset).wait_send()


def on_device(
    block_source_tensor,
    attend_initial_norm_gain,
    each_channel_group_norm,
    attend_final_norm_gain,
    dense_initial_norm_gain,
    dense_final_norm_gain,
    question_map,
    address_map,
    payload_weights_map,
    fading_left_factor,
    fading_right_factor,
    fading_valve_constant,
    sudden_fade_excess,
    combining_map,
    valve_map,
    widening_map,
    valve_conv_stencil,
    widening_conv_stencil,
    narrowing_map,
):
    line, parts, ranks = lax.axis_size("fs"), lax.axis_size("grp"), lax.axis_size("tp")
    length, own = block_source_tensor.shape
    chips = ranks // 2
    width = own * ranks
    shards = (
        question_map,
        address_map,
        payload_weights_map,
        combining_map,
        valve_map,
        widening_map,
        narrowing_map,
    )
    cuts = [cuts_of(shard, parts) for shard in shards]
    down_wide = narrowing_map.shape[1]
    down_cuts = 1
    while down_wide == own and down_cuts < cuts[6] and down_wide % (down_cuts * 2 * 128) == 0:
        down_cuts *= 2
    cuts[6] = down_cuts
    units = sum(cuts)
    turns = 1 + down_cuts
    down_own = own // down_cuts
    hidden_units = valve_map.shape[1]
    head_count = each_channel_group_norm.shape[0]

    def full(shard, dimension):
        rows, columns = shard.shape
        shape = (rows * line, columns) if dimension == 0 else (rows, columns * line)
        return pltpu.VMEM(shape, bf16)

    dma = pltpu.SemaphoreType.DMA
    scratch = [full(shard, dimension) for shard, dimension in zip(shards, (0, 0, 0, 1, 0, 0, 1))]
    scratch += [
        pltpu.VMEM((length, width), bf16),
        pltpu.VMEM((length, width), bf16),
        pltpu.VMEM((length, width), bf16),
        pltpu.VMEM((length, question_map.shape[1]), bf16),
        pltpu.VMEM((length, address_map.shape[1]), bf16),
        pltpu.VMEM((length, payload_weights_map.shape[1]), bf16),
        pltpu.VMEM((length, fading_left_factor.shape[1]), f32),
        pltpu.VMEM((length, payload_weights_map.shape[1]), bf16),
        pltpu.VMEM((head_count, VALUE_DIM, KEY_DIM), f32),
    ]
    scratch += [pltpu.VMEM((ranks, length, own), bf16)]
    scratch += [pltpu.VMEM((chips, length, own), bf16)] * 3
    scratch += [
        pltpu.VMEM((length, own), f32),
        pltpu.VMEM((8, length), f32),
        pltpu.VMEM((ranks, 8, length), f32),
        pltpu.VMEM((length, own), bf16),
    ]
    scratch += [
        pltpu.VMEM((length + 8, tile_of(hidden_units)), f32),
        pltpu.VMEM((length, hidden_units), f32),
        pltpu.VMEM((length, hidden_units), bf16),
        pltpu.VMEM((down_cuts, ranks, length, down_own), bf16),
    ]
    scratch += [pltpu.VMEM((down_cuts, chips, length, down_own), bf16)] * 3
    scratch += [
        pltpu.VMEM((length, own), f32),
        pltpu.VMEM((8, length), f32),
        pltpu.VMEM((ranks, 8, length), f32),
    ]
    scratch += [dma((7,))] + [dma((units, 2, line))] * 2
    scratch += [dma((units, 2, line, max(parts - 1, 1)))] * 2
    scratch += [dma((2,))] + [dma((2, ranks))] * 2
    scratch += [dma((turns, chips))] * 4 + [dma((2, ranks))] * 2
    vmem, anywhere = pl.BlockSpec(memory_space=pltpu.VMEM), pl.BlockSpec(memory_space=pl.ANY)
    return pl.pallas_call(
        functools.partial(layer_kernel, (tuple(cuts), down_cuts, line, parts, ranks)),
        out_shape=jax.ShapeDtypeStruct((length, own), bf16),
        in_specs=[vmem] * 12 + [anywhere] * 7,
        out_specs=vmem,
        scratch_shapes=scratch,
        compiler_params=pltpu.CompilerParams(
            collective_id=1, has_side_effects=True, vmem_limit_bytes=60 * 1024 * 1024
        ),
    )(
        block_source_tensor,
        attend_initial_norm_gain[None],
        each_channel_group_norm,
        attend_final_norm_gain[None],
        dense_initial_norm_gain[None],
        dense_final_norm_gain[None],
        fading_left_factor,
        fading_right_factor,
        fading_valve_constant[None],
        sudden_fade_excess,
        valve_conv_stencil,
        widening_conv_stencil,
        *shards,
    )


def solution(mesh):
    placed = (
        P(("grp", "fs"), "tp"),
        P(),
        P("tp", None),
        P(),
        P(),
        P(),
        P("fs", "tp"),
        P("fs", "tp"),
        P("fs", "tp"),
        P(),
        P(None, "tp"),
        P("tp"),
        P(("grp", "fs"), "tp"),
        P("tp", "fs"),
        P("fs", "tp"),
        P("fs", "tp"),
        P(None, "tp"),
        P(None, "tp"),
        P("tp", "fs"),
    )
    return jax.shard_map(
        on_device, mesh=mesh, in_specs=placed, out_specs=P(("grp", "fs"), "tp"), check_vma=False
    )
```

time: 232 us -> 180 us (0.78)
  matrix products: 21.8 us -> 0 us
  Pallas kernels: 197 us -> 176 us
  other arithmetic: 11.2 us -> 0 us
    dot_general x8 -> x0, matrix products: 21.8 us -> none  [the longest x3 6.75 us: on_device(): jnp.dot(normed, full, preferred_element_type=jnp.float32)]
    pallas_call x5 -> x1, Pallas kernels: 197 us -> 176 us  [on_device(): pl.pallas_call(functools.partial(layer_kernel, (tuple(cuts), down_cuts, l...]
    convert_element_type x4 -> x0, other arithmetic: 4.49 us -> none  [the longest x1 2.24 us: on_device(): return (first.astype(jnp.float32) + channel * lax.rsqrt(channel_squares[:...]
    reduce_sum x2 -> x0, other arithmetic: 4.45 us -> none  [norm_rows(): jnp.mean(values * values, axis=-1, keepdims=True) + epsilon]
    unnamed x28 -> x2, local copies, waits for them, and re-layouts: 0.06 us -> 3.71 us
where the time goes in v1:
time: 180 us
  Pallas kernels  176 us (98%)
  local copies, waits for them, and re-layouts  3.71 us (2%)
    pallas_call x1, Pallas kernels, on_device(): pl.pallas_call(functools.partial(layer_kernel, (tuple(cuts), down_cuts, l...  176 us
    unnamed x2, local copies, waits for them, and re-layouts  3.71 us

profile of v1, /device:TPU:0, one launch (start us, length us, event | category | flops | bytes accessed | tf_op | source)
XLA Modules:
  0.0 179.9 jit_solution(16999954766802925470)
XLA Ops:
  0.0 1.8 %copy.20.refs_6_ = bf16[2048,16]{1,0:T(8,128)(2,1)} copy(bf16[2048,16]{0,1:T(8,128)(2,1)} %param.28) | data formatting | bytes 131072 | tf_op args[9]
  1.8 176.1 %shard_map.181 = bf16[512,512]{1,0:T(8,128)(2,1)} custom-call(bf16[512,512]{1,0:T(8,128)(2,1)} %refs_0_.1, f32[1,2048]{1,0:T(1,128)} %bitcast.5, f32[2,256]{1,0:T(2,128)} %refs_2_.1, f32[1,2048]{1,0:T(1,128)} %bitcast.6, f32[1,2048]{1,0:T(1,128)} %bitcast.7, f32[1,2048]{1,0:T(1,128)} %bitcast.8, bf16[2048,16]{1,0:T(8,128)(2,1)} %copy.20.refs_6_, ...), custom_call_target="tpu_custom_call" | custom-call | tf_op jit(solution)/shard_map/pallas_call | solution.py:738
  178.0 1.9 %copy.22 = bf16[512,512]{1,0:T(8,128)(2,1)} copy(bf16[512,512]{1,0:T(8,128)(2,1)} %shard_map.181) | data formatting | bytes 1048576

commit v2 on v1

--- a/solution.py
+++ b/solution.py
@@ -20,7 +20,8 @@
 f32, bf16 = jnp.float32, jnp.bfloat16
 
 AHEAD = 2
-STEP_BUDGET = 4.5
+STEP_BUDGET = 2.0
+LAG = 1
 
 
 def norm_rows(values, channel_gain):
@@ -65,7 +66,7 @@
 
 
 def layer_kernel(config, *refs):
-    cuts, down_cuts, line, parts, ranks = config
+    cuts, down_cuts, evened, line, parts, ranks = config
     refs = list(refs)
 
     def take(number):
@@ -73,16 +74,18 @@
         del refs[:number]
         return taken
 
-    block, first_gain, head_gain, mixed_gain, second_gain, last_gain = take(6)
-    left, right, valve, excess, gate_taps, up_taps = take(6)
+    first_gain, head_gain, mixed_gain, second_gain, last_gain = take(5)
+    left, right, valve, gate_taps, up_taps = take(5)
+    block_in, excess_in = take(2)
     shards = take(7)
     (out,) = take(1)
     maps = take(7)
+    block, excess = take(2)
     rows_full, first_full, normed, query, key, value, low, head_out, states = take(9)
     partial, pair_in, chip_sum, chip_in, total, squares_own, squares_in, first = take(8)
     padded, gate_act, hidden, down_partial, down_pair, down_sum, down_in, down_total = take(8)
     down_squares_own, down_squares_in = take(2)
-    own_sem, line_send, line_recv, part_send, part_recv = take(5)
+    own_sem, input_sem, line_send, line_recv, part_send, part_recv = take(6)
     spread_own, spread_send, spread_recv = take(3)
     pair_send, pair_recv, chip_send, chip_recv, squares_send, squares_recv = take(6)
 
@@ -101,9 +104,19 @@
     units = []
     for which in range(7):
         for cut in range(cuts[which]):
-            units.append((which, cut))
+            units.append((which, cut, None))
+    if evened:
+        units += [(6, down_cuts - 1, half) for half in range(parts)]
     unit_count = len(units)
-    first_unit = [sum(cuts[:which]) for which in range(8)]
+
+    def last_unit(which, cut):
+        return max(index for index, unit in enumerate(units) if unit[:2] == (which, cut))
+
+    def in_last_cut(unit):
+        return evened and units[unit][:2] == (6, down_cuts - 1)
+
+    def send_row(unit):
+        return 7 if in_last_cut(unit) else units[unit][0]
 
     def there(way):
         return place < line - 1 if way == 0 else place > 0
@@ -118,12 +131,17 @@
         return lax.rem(part + offset, parts)
 
     def at(full, unit, owner, half):
-        which, cut = units[unit]
+        which, cut, fixed = units[unit]
+        half = half if fixed is None else fixed
         ref = maps[which] if full else shards[which]
         shard_rows, shard_columns = shards[which].shape
         if which == 6:
             height, wide = shard_rows // parts, shard_columns // cuts[which]
+            if in_last_cut(unit):
+                height //= 2
             row, column = half * height, cut * wide
+            if fixed is not None:
+                row = shard_rows // 2 + fixed * height
             if full:
                 column = owner * shard_columns + cut * wide
         else:
@@ -148,37 +166,76 @@
             device_id_type=MESH,
         )
 
+    def sent_by(way, step):
+        return place - step if way == 0 else place + step
+
+    def coming_from(way, step):
+        return sent_by(way, step + 1)
+
+    def seat(way, owner):
+        return owner - 1 if way else owner
+
     def first_copy(unit, way):
         return remote(
             at(False, unit, place, part),
             at(True, unit, place, part),
-            line_send.at[unit, way, 0],
-            line_recv.at[unit, way, 0],
+            line_send.at[send_row(unit), line if way else place],
+            line_recv.at[unit, seat(way, place)],
             toward(way),
         )
 
     def line_copy(unit, way, step):
-        target = at(True, unit, place - step if way == 0 else place + step, part)
+        owner = sent_by(way, step)
+        target = at(True, unit, owner, part)
         return remote(
-            target, target, line_send.at[unit, way, step], line_recv.at[unit, way, step], toward(way)
+            target, target, line_send.at[send_row(unit), owner], line_recv.at[unit, seat(way, owner)], toward(way)
         )
 
     def arrival(unit, way, step):
-        target = at(True, unit, place - step - 1 if way == 0 else place + step + 1, part)
+        owner = coming_from(way, step)
+        target = at(True, unit, owner, part)
         return remote(
-            target, target, line_send.at[unit, way, step], line_recv.at[unit, way, step], toward(way)
-        )
-
-    def part_copy(unit, way, step, offset, coming):
-        mine = part_of(parts - offset) if coming else part
-        target = at(True, unit, place - step - 1 if way == 0 else place + step + 1, mine)
+            target, target, line_send.at[send_row(unit), owner], line_recv.at[unit, seat(way, owner)], toward(way)
+        )
+
+    def part_copy(unit, way, step, offset):
+        owner = coming_from(way, step)
+        target = at(True, unit, owner, part)
         return remote(
             target,
             target,
-            part_send.at[unit, way, step, offset - 1],
-            part_recv.at[unit, way, step, offset - 1],
+            part_send.at[send_row(unit), owner, offset - 1],
+            part_recv.at[unit, offset - 1],
             {"grp": part_of(offset)},
         )
+
+    def sent_of(row, owner, over_line):
+        ref = maps[min(row, 6)]
+        shard_rows, shard_columns = shards[min(row, 6)].shape
+        height = shard_rows // parts
+        if row == 7:
+            wide = shard_columns // down_cuts
+            height //= 2
+            return ref.at[
+                0 : height + (shard_rows // 2 if over_line else 0),
+                pl.ds(pl.multiple_of(owner * shard_columns + shard_columns - wide, wide), wide),
+            ]
+        rows = pl.ds(pl.multiple_of(part * height, height), height)
+        if row == 6 and evened:
+            wide = shard_columns // down_cuts
+            return ref.at[
+                rows,
+                pl.ds(pl.multiple_of(owner * shard_columns, wide), shard_columns - wide),
+            ]
+        if row == 3 or row == 6:
+            return ref.at[
+                rows, pl.ds(pl.multiple_of(owner * shard_columns, shard_columns), shard_columns)
+            ]
+        return ref.at[pl.ds(pl.multiple_of(owner * shard_rows + part * height, height), height), :]
+
+    def sent_part(row, owner, sem, device, over_line):
+        target = sent_of(row, owner, over_line)
+        return remote(target, target, sem, line_recv.at[0, 0], device)
 
     def own_copy(which):
         height, wide = shards[which].shape
@@ -208,67 +265,114 @@
                     def _():
                         line_copy(unit, way, step + 1).start()
 
-                for offset in range(1, parts):
-                    part_copy(unit, way, step, offset, False).start()
+                if units[unit][2] is None:
+                    for offset in range(1, parts):
+                        part_copy(unit, way, step, offset).start()
 
     def finish(unit):
+        if units[unit][2] is not None:
+            return
+        which = units[unit][0]
+        height, wide = at(True, unit, 0, 0).shape
+        if which in (3, 6):
+            everything = maps[which].at[0:height, 0 : (line - 1) * wide]
+        else:
+            everything = maps[which].at[0 : (line - 1) * height, :]
+        for offset in range(1, parts):
+            remote(
+                everything,
+                everything,
+                part_send.at[which, 0, offset - 1],
+                part_recv.at[unit, offset - 1],
+                {"grp": part_of(offset)},
+            ).wait_recv()
+
+    def drain(which):
+        for way in range(2):
+
+            @pl.when(there(way))
+            def _():
+                sent_part(
+                    which, place, line_send.at[which, line if way else place], toward(way), True
+                ).wait_send()
+
         @pl.loop(0, line - 1)
         def _(step):
             for way in range(2):
 
                 @pl.when(comes(way, step))
                 def _():
-                    for offset in range(1, parts):
-                        part_copy(unit, way, step, offset, True).wait_recv()
-
-    def drain(unit):
-        for way in range(2):
-
-            @pl.when(there(way))
-            def _():
-                first_copy(unit, way).wait_send()
-
-        @pl.loop(0, line - 1)
-        def _(step):
-            for way in range(2):
-
-                @pl.when(comes(way, step))
-                def _():
+                    owner = coming_from(way, step)
+
                     @pl.when(there(way))
                     def _():
-                        line_copy(unit, way, step + 1).wait_send()
+                        sent_part(
+                            which, owner, line_send.at[which, owner], toward(way), True
+                        ).wait_send()
 
                     for offset in range(1, parts):
-                        part_copy(unit, way, step, offset, False).wait_send()
+                        sent_part(
+                            which,
+                            owner,
+                            part_send.at[which, owner, offset - 1],
+                            {"grp": part_of(offset)},
+                            False,
+                        ).wait_send()
 
     def columns_of(ref, owner):
         return ref.at[:, pl.ds(pl.multiple_of(owner * own, own), own)]
 
-    def spread_copy(turn, source, full, offset, owner):
+    def spread_copy(turn, source, full, slot, owner, target):
         return remote(
             source,
             columns_of(full, owner),
-            spread_send.at[turn, offset],
-            spread_recv.at[turn, offset],
-            {"tp": rank_at(offset)},
+            spread_send.at[turn, slot],
+            spread_recv.at[turn, slot],
+            {"tp": target},
+        )
+
+    def chip_at(offset):
+        return lax.rem(chip + offset, chips) * 2
+
+    def sibling_copy(turn, source, full, coming):
+        owner = chip * 2 + 1 - core if coming else rank
+        return spread_copy(turn, source, full, 0, owner, chip * 2 + 1 - core)
+
+    def across_copy(turn, source, full, offset, coming):
+        owner = chip_at(chips - offset) + core if coming else rank
+        return spread_copy(turn, source, full, offset, owner, chip_at(offset) + core)
+
+    def relay_copy(turn, full, offset, coming):
+        owner = chip_at(chips - offset) + (1 - core if coming else core)
+        return spread_copy(
+            turn, columns_of(full, owner), full, chips - 1 + offset, owner, chip * 2 + 1 - core
         )
 
     def spread_local(turn, source, full):
         return pltpu.make_async_copy(source, columns_of(full, rank), spread_own.at[turn])
 
     def spread_start(turn, source, full):
-        for offset in range(1, ranks):
-            spread_copy(turn, source, full, offset, rank).start()
+        for offset in range(1, chips):
+            across_copy(turn, source, full, offset, False).start()
+        sibling_copy(turn, source, full, False).start()
         spread_local(turn, source, full).start()
+
+    def spread_relay(turn, source, full):
+        for offset in range(1, chips):
+            across_copy(turn, source, full, offset, True).wait_recv()
+            relay_copy(turn, full, offset, False).start()
 
     def spread_wait(turn, source, full):
         spread_local(turn, source, full).wait()
-        for offset in range(1, ranks):
-            spread_copy(turn, source, full, offset, rank_at(ranks - offset)).wait_recv()
+        sibling_copy(turn, source, full, True).wait_recv()
+        for offset in range(1, chips):
+            relay_copy(turn, full, offset, True).wait_recv()
 
     def spread_drain(turn, source, full):
-        for offset in range(1, ranks):
-            spread_copy(turn, source, full, offset, rank).wait_send()
+        sibling_copy(turn, source, full, False).wait_send()
+        for offset in range(1, chips):
+            across_copy(turn, source, full, offset, False).wait_send()
+            relay_copy(turn, full, offset, False).wait_send()
 
     def sum_refs(turn):
         if turn == 0:
@@ -338,15 +442,19 @@
             {"tp": rank_at(offset)},
         )
 
-    def squares_start(turn, values_ref):
-        values = values_ref[...]
-        (squares_own, down_squares_own)[turn][...] = lax.dot_general(
-            jnp.ones((8, own), f32),
+    def squares_add(turn, result, again):
+        values = result[...]
+        squares = lax.dot_general(
+            jnp.ones((8, values.shape[1]), f32),
             values * values,
             (((1,), (1,)), ((), ())),
             precision=careful_evaluation,
             preferred_element_type=f32,
         )
+        target = (squares_own, down_squares_own)[turn]
+        target[...] = target[...] + squares if again else squares
+
+    def squares_start(turn):
         for offset in range(1, ranks):
             squares_copy(turn, offset).start()
 
@@ -365,35 +473,29 @@
         )
         return lax.rsqrt(columns[:, :1] / width + epsilon)
 
-    def norm_into(source, gain):
-        tall = 64
+    norm_step = length // 4
+
+    def norm_part(source, gain, start):
+        tall = min(64, norm_step)
 
         def one(index, carry):
-            rows = pl.ds(pl.multiple_of(index * tall, tall), tall)
+            rows = pl.ds(pl.multiple_of(start + index * tall, tall), tall)
             normed[rows, :] = norm_rows(source[rows, :].astype(f32), gain[...]).astype(bf16)
             return carry
 
-        lax.fori_loop(0, length // tall, one, 0)
-
-    def over_columns(ref_width, body):
-        wide = tile_of(ref_width)
-
-        def one(index, carry):
-            body(pl.ds(pl.multiple_of(index * wide, wide), wide))
-            return carry
-
-        lax.fori_loop(0, ref_width // wide, one, 0)
-
-    def project(which, target):
-        def body(columns):
-            target[:, columns] = jnp.dot(
-                normed[...], maps[which][:, columns], preferred_element_type=f32
-            ).astype(bf16)
-
-        over_columns(maps[which].shape[1], body)
+        lax.fori_loop(0, norm_step // tall, one, 0)
+
+    def tiles_of(total_width):
+        wide = tile_of(total_width)
+        return [pl.ds(index * wide, wide) for index in range(total_width // wide)]
+
+    def project(which, target, columns):
+        target[:, columns] = jnp.dot(
+            normed[...], maps[which][:, columns], preferred_element_type=f32
+        ).astype(bf16)
 
     def low_rank():
-        low[...] = jnp.dot(normed[...], left[...], preferred_element_type=f32)
+        low[...] = contract(normed[...], left[...], 1, 1)
 
     def one_chunk(index, carried):
         rows = lax.broadcasted_iota(jnp.int32, (CHUNK, CHUNK), 0)
@@ -457,29 +559,30 @@
         return tuple(after)
 
     chunk_count = length // CHUNK
-    chunk_step = max(1, chunk_count // 4)
+    chunk_step = 1
 
     def mix(start):
         if start == 0:
             carried = tuple(jnp.zeros((VALUE_DIM, KEY_DIM), f32) for _ in range(head_count))
         else:
             carried = tuple(states[head] for head in range(head_count))
-        carried = lax.fori_loop(start, min(start + chunk_step, chunk_count), one_chunk, carried)
+        carried = one_chunk(start, carried)
         for head in range(head_count):
             states[head] = carried[head]
 
-    def combine():
-        for target in range(ranks):
-
-            def body(columns, target=target):
-                columns_full = pl.ds(
-                    pl.multiple_of(target * own + columns.start, columns.size), columns.size
-                )
-                partial[target, :, columns] = jnp.dot(
-                    head_out[...], maps[3][:, columns_full], preferred_element_type=f32
-                ).astype(bf16)
-
-            over_columns(own, body)
+    def combine(index):
+        target = lax.rem(rank + 2 + index, ranks)
+
+        def body(step, carry):
+            wide = tile_of(own)
+            columns = pl.ds(pl.multiple_of(step * wide, wide), wide)
+            columns_full = pl.ds(pl.multiple_of(target * own + step * wide, wide), wide)
+            partial[target, :, columns] = jnp.dot(
+                head_out[...], maps[3][:, columns_full], preferred_element_type=f32
+            ).astype(bf16)
+            return carry
+
+        lax.fori_loop(0, own // tile_of(own), body, 0)
 
     def start_pairs(turn):
         for target in range(chips):
@@ -504,39 +607,40 @@
 
     padded_rows = padded.shape[0] - length
 
-    def gate():
+    def gate(columns):
         padded[0:padded_rows, :] = jnp.zeros((padded_rows, padded.shape[1]), f32)
-
-        def body(columns):
-            padded[padded_rows:, :] = jnp.dot(
-                normed[...], maps[4][:, columns], preferred_element_type=f32
-            )
-            turned = taps(gate_taps, columns)
-            gate_act[:, columns] = turned / (1.0 + jnp.exp(-turned))
-
-        over_columns(maps[4].shape[1], body)
-
-    def up():
-        def body(columns):
-            padded[padded_rows:, :] = jnp.dot(
-                normed[...], maps[5][:, columns], preferred_element_type=f32
-            )
-            hidden[:, columns] = (gate_act[:, columns] * taps(up_taps, columns)).astype(bf16)
-
-        over_columns(maps[5].shape[1], body)
+        padded[padded_rows:, :] = jnp.dot(
+            normed[...], maps[4][:, columns], preferred_element_type=f32
+        )
+        turned = taps(gate_taps, columns)
+        gate_act[:, columns] = turned / (1.0 + jnp.exp(-turned))
+
+    def up(columns):
+        padded[padded_rows:, :] = jnp.dot(
+            normed[...], maps[5][:, columns], preferred_element_type=f32
+        )
+        hidden[:, columns] = (gate_act[:, columns] * taps(up_taps, columns)).astype(bf16)
 
     def down(unit):
         wide = own // down_cuts
-
-        def one(target, carry):
-            columns = pl.ds(pl.multiple_of(target * own + unit * wide, wide), wide)
-            down_partial[unit, target] = jnp.dot(
-                hidden[...], maps[6][:, columns], preferred_element_type=f32
+        group = 2 if wide == 128 and chips % 2 == 0 else 1
+
+        def some(who, index):
+            targets = [(index * group + each) * 2 + who for each in range(group)]
+            columns = [pl.ds(pl.multiple_of(target * own + unit * wide, wide), wide) for target in targets]
+            product = jnp.dot(
+                hidden[...],
+                jnp.concatenate([maps[6][:, each] for each in columns], axis=1),
+                preferred_element_type=f32,
             ).astype(bf16)
-            return carry
-
-        lax.fori_loop(0, ranks, one, 0)
-        start_pairs(1 + unit)
+            for each, target in enumerate(targets):
+                down_partial[unit, target] = product[:, each * wide : (each + 1) * wide]
+
+        for who in (1 - core, core):
+            for index in range(chips // group):
+                some(who, index)
+            if who is not core:
+                start_pairs(1 + unit)
 
     def last():
         scale = squares_wait(1)
@@ -561,7 +665,13 @@
 
     for unit in range(min(AHEAD, unit_count)):
         begin(unit)
-    spread_start(0, block, rows_full)
+    spread_start(0, block_in, rows_full)
+    inputs = [
+        pltpu.make_async_copy(source, target, input_sem.at[index])
+        for index, (source, target) in enumerate(((block_in, block), (excess_in, excess)))
+    ]
+    for copy in inputs:
+        copy.start()
     for which in range(7):
         own_copy(which).start()
 
@@ -569,33 +679,54 @@
     landed = [0]
     loaded = set()
 
-    def job(needs, gap, cost, *work):
+    def job(needs, gap, cost, work):
         jobs.append((needs, gap, cost, work))
 
     def whole(which):
-        return first_unit[which + 1] - 1
-
-    job(-1, 2, 3.0, lambda: spread_wait(0, block, rows_full), lambda: norm_into(rows_full, first_gain), low_rank)
-    job(whole(0), 0, 1.5, lambda: project(0, query))
-    job(whole(1), 0, 1.5, lambda: project(1, key))
-    job(whole(2), 0, 3.5, lambda: project(2, value))
+        return last_unit(which, cuts[which] - 1)
+
+    job(-1, 6, 0.2, lambda: spread_relay(0, block_in, rows_full))
+    job(-1, 1, 0.2, lambda: spread_wait(0, block_in, rows_full))
+    for start in range(0, length, norm_step):
+        job(-1, 0, 0.6, functools.partial(norm_part, rows_full, first_gain, start))
+    job(-1, 0, 0.6, low_rank)
+    for which, target in ((0, query), (1, key), (2, value)):
+        for columns in tiles_of(maps[which].shape[1]):
+            job(whole(which), 0, 1.2, functools.partial(project, which, target, columns))
+    job(whole(2), 0, 0.1, lambda: [copy.wait() for copy in inputs])
     for start in range(0, chunk_count, chunk_step):
-        job(whole(2), 0, 3.0, functools.partial(mix, start))
-    job(whole(3), 0, 4.0, combine, lambda: start_pairs(0))
-    job(-1, 1, 2.0, lambda: sum_pairs(0))
-    job(-1, 2, 2.0, lambda: sum_chips(0), lambda: squares_start(0, total))
-    job(-1, 1, 2.0, make_first)
-    job(-1, 3, 2.5, lambda: spread_wait(1, first, first_full), lambda: norm_into(first_full, second_gain))
-    job(whole(4), 0, 4.5, gate)
-    job(whole(5), 0, 4.5, up)
+        job(whole(2), 0, 1.2, functools.partial(mix, start))
+    for index in range(ranks):
+        job(whole(3), 0, 0.7, functools.partial(combine, index))
+    job(whole(3), 0, 0.1, lambda: start_pairs(0))
+    job(-1, 1, 1.2, lambda: sum_pairs(0))
+    job(-1, 6, 0.4, lambda: sum_chips(0))
+    job(-1, 0, 1.0, lambda: squares_add(0, total, False))
+    job(-1, 0, 0.1, lambda: squares_start(0))
+    job(-1, 1, 0.9, make_first)
+    job(-1, 6, 0.2, lambda: spread_relay(1, first, first_full))
+    job(-1, 1, 0.2, lambda: spread_wait(1, first, first_full))
+    for start in range(0, length, norm_step):
+        job(-1, 0, 0.6, functools.partial(norm_part, first_full, second_gain, start))
+    for columns in tiles_of(maps[4].shape[1]):
+        job(whole(4), 0, 1.0, functools.partial(gate, columns))
+    for columns in tiles_of(maps[5].shape[1]):
+        job(whole(5), 0, 1.0, functools.partial(up, columns))
+
+    def take_sum(unit):
+        sum_chips(1 + unit)
+        squares_add(1, sum_refs(1 + unit)[4], unit > 0)
+
     for unit in range(down_cuts):
-        job(first_unit[6] + unit, 0, 1.0, functools.partial(down, unit))
+        if unit >= 3:
+            job(-1, 0, 0.6, functools.partial(take_sum, unit - 3))
+        job(last_unit(6, unit), 0, 1.2, functools.partial(down, unit))
         if unit:
-            job(-1, 0, 1.0, functools.partial(sum_pairs, unit))
-    job(-1, 0, 1.0, functools.partial(sum_pairs, down_cuts))
-    for unit in range(down_cuts):
-        job(-1, 0, 0.5, functools.partial(sum_chips, 1 + unit))
-    job(-1, 0, 1.0, lambda: squares_start(1, down_total))
+            job(-1, 0, 0.6, functools.partial(sum_pairs, unit))
+    job(-1, 0, 0.6, functools.partial(sum_pairs, down_cuts))
+    for unit in range(max(down_cuts - 3, 0), down_cuts):
+        job(-1, 0, 0.6, functools.partial(take_sum, unit))
+    job(-1, 0, 0.1, lambda: squares_start(1))
     job(-1, 0, 1.0, last)
 
     def land(needs):
@@ -608,36 +739,35 @@
             finish(unit)
             landed[0] += 1
 
-    at_step = -1
-    spent = 0.0
     previous = 0
+    slot = 0
     for tick in range(unit_count + line - 2):
         if tick + AHEAD < unit_count:
             begin(tick + AHEAD)
         for step in range(line - 1):
             if 0 <= tick - step < unit_count:
                 pass_on(tick - step, step)
-        spent = 0.0
-        while jobs:
-            needs, gap, cost, work = jobs[0]
-            if spent + cost > STEP_BUDGET and spent > 0.0:
-                break
-            if tick < needs + line - 1 or tick < previous + gap:
-                break
-            jobs.pop(0)
-            land(needs)
-            for act in work:
-                act()
-            spent += cost
-            previous = tick
+                slot += 1
+            spent = 0.0
+            while jobs:
+                needs, gap, cost, work = jobs[0]
+                if spent > 0.0 and spent + cost > STEP_BUDGET:
+                    break
+                lag = LAG if needs < 0 or units[needs][2] is None else 0
+                if tick < needs + line - 1 + lag or slot < previous + gap:
+                    break
+                jobs.pop(0)
+                land(needs)
+                work()
+                spent += cost
+                previous = slot
     for needs, _, _, work in jobs:
         land(needs)
-        for act in work:
-            act()
-
-    for unit in range(unit_count):
-        drain(unit)
-    spread_drain(0, block, rows_full)
+        work()
+
+    for which in range(8 if evened else 7):
+        drain(which)
+    spread_drain(0, block_in, rows_full)
     spread_drain(1, first, first_full)
     for turn in range(1 + down_cuts):
         sums_drain(turn)
@@ -686,7 +816,10 @@
     while down_wide == own and down_cuts < cuts[6] and down_wide % (down_cuts * 2 * 128) == 0:
         down_cuts *= 2
     cuts[6] = down_cuts
-    units = sum(cuts)
+    if question_map.shape[0] % (parts * cuts[0] * 2 * 16) == 0:
+        cuts[0] *= 2
+    evened = down_cuts > 1 and narrowing_map.shape[0] % (2 * parts * 16) == 0
+    units = sum(cuts) + (parts if evened else 0)
     turns = 1 + down_cuts
     down_own = own // down_cuts
     hidden_units = valve_map.shape[1]
@@ -700,6 +833,8 @@
     dma = pltpu.SemaphoreType.DMA
     scratch = [full(shard, dimension) for shard, dimension in zip(shards, (0, 0, 0, 1, 0, 0, 1))]
     scratch += [
+        pltpu.VMEM(block_source_tensor.shape, bf16),
+        pltpu.VMEM(sudden_fade_excess.shape, f32),
         pltpu.VMEM((length, width), bf16),
         pltpu.VMEM((length, width), bf16),
         pltpu.VMEM((length, width), bf16),
@@ -730,33 +865,33 @@
         pltpu.VMEM((8, length), f32),
         pltpu.VMEM((ranks, 8, length), f32),
     ]
-    scratch += [dma((7,))] + [dma((units, 2, line))] * 2
-    scratch += [dma((units, 2, line, max(parts - 1, 1)))] * 2
+    scratch += [dma((7,)), dma((2,)), dma((8, line + 1)), dma((units, line - 1))]
+    scratch += [dma((8, line, max(parts - 1, 1))), dma((units, max(parts - 1, 1)))]
     scratch += [dma((2,))] + [dma((2, ranks))] * 2
     scratch += [dma((turns, chips))] * 4 + [dma((2, ranks))] * 2
     vmem, anywhere = pl.BlockSpec(memory_space=pltpu.VMEM), pl.BlockSpec(memory_space=pl.ANY)
     return pl.pallas_call(
-        functools.partial(layer_kernel, (tuple(cuts), down_cuts, line, parts, ranks)),
+        functools.partial(layer_kernel, (tuple(cuts), down_cuts, evened, line, parts, ranks)),
         out_shape=jax.ShapeDtypeStruct((length, own), bf16),
-        in_specs=[vmem] * 12 + [anywhere] * 7,
+        in_specs=[vmem] * 10 + [anywhere] * 9,
         out_specs=vmem,
         scratch_shapes=scratch,
         compiler_params=pltpu.CompilerParams(
             collective_id=1, has_side_effects=True, vmem_limit_bytes=60 * 1024 * 1024
         ),
     )(
-        block_source_tensor,
         attend_initial_norm_gain[None],
         each_channel_group_norm,
         attend_final_norm_gain[None],
         dense_initial_norm_gain[None],
         dense_final_norm_gain[None],
-        fading_left_factor,
+        fading_left_factor.T,
         fading_right_factor,
         fading_valve_constant[None],
-        sudden_fade_excess,
         valve_conv_stencil,
         widening_conv_stencil,
+        block_source_tensor,
+        sudden_fade_excess,
         *shards,
     )
 

time: 180 us -> 159 us (0.88)
  Pallas kernels: 176 us -> 157 us
  local copies, waits for them, and re-layouts: 3.71 us -> 1.87 us
    pallas_call x1, Pallas kernels: 176 us -> 157 us  [on_device(): pl.pallas_call(functools.partial(layer_kernel, (tuple(cuts), down_cuts, e...]
    unnamed x2 -> x1, local copies, waits for them, and re-layouts: 3.71 us -> 1.87 us
where the time goes in v2:
time: 159 us
  Pallas kernels  157 us (99%)
  local copies, waits for them, and re-layouts  1.87 us (1%)
    pallas_call x1, Pallas kernels, on_device(): pl.pallas_call(functools.partial(layer_kernel, (tuple(cuts), down_cuts, e...  157 us

profile of v2, /device:TPU:0, one launch (start us, length us, event | category | flops | bytes accessed | tf_op | source)
XLA Modules:
  0.0 159.0 jit_solution(4214628809760815519)
XLA Ops:
  0.0 157.1 %shard_map.181 = bf16[512,512]{1,0:T(8,128)(2,1)} custom-call(f32[1,2048]{1,0:T(1,128)} %bitcast.7, f32[2,256]{1,0:T(2,128)} %refs_1_.1, f32[1,2048]{1,0:T(1,128)} %bitcast.8, f32[1,2048]{1,0:T(1,128)} %bitcast.9, f32[1,2048]{1,0:T(1,128)} %bitcast.10, bf16[16,2048]{1,0:T(8,128)(2,1)} %bitcast.6, f32[16,256]{1,0:T(8,128)} %refs_6_.1, f32[1,256]{1,0:T(1,128)} %bitcast.11, ...), custom_call_target="tpu_custom_call" | custom-call | tf_op jit(solution)/shard_map/pallas_call | solution.py:873
  157.1 1.9 %copy.21 = bf16[512,512]{1,0:T(8,128)(2,1)} copy(bf16[512,512]{1,0:T(8,128)(2,1)} %shard_map.181) | data formatting | bytes 1048576

commit v3 on v2

--- a/solution.py
+++ b/solution.py
@@ -20,8 +20,10 @@
 f32, bf16 = jnp.float32, jnp.bfloat16
 
 AHEAD = 2
+SHIFT = 1
+FADING = False
 STEP_BUDGET = 2.0
-LAG = 1
+LAG = 3
 
 
 def norm_rows(values, channel_gain):
@@ -84,8 +86,8 @@
     rows_full, first_full, normed, query, key, value, low, head_out, states = take(9)
     partial, pair_in, chip_sum, chip_in, total, squares_own, squares_in, first = take(8)
     padded, gate_act, hidden, down_partial, down_pair, down_sum, down_in, down_total = take(8)
-    down_squares_own, down_squares_in = take(2)
-    own_sem, input_sem, line_send, line_recv, part_send, part_recv = take(6)
+    down_squares_own, down_squares_in, result = take(3)
+    out_sem, own_sem, input_sem, line_send, line_recv, part_send, part_recv = take(7)
     spread_own, spread_send, spread_recv = take(3)
     pair_send, pair_recv, chip_send, chip_recv, squares_send, squares_recv = take(6)
 
@@ -407,18 +409,20 @@
             {"tp": lax.rem(chip + offset, chips) * 2 + core},
         )
 
+    def sum_pair(turn, offset):
+        source, landing, sums, _, result = sum_refs(turn)
+        target = lax.rem(chip + offset, chips)
+        pair_copy(turn, target).wait_recv()
+        both = source[target * 2 + core].astype(f32) + landing[target].astype(f32)
+        if offset:
+            sums[offset] = both.astype(bf16)
+            chip_copy(turn, offset).start()
+        else:
+            result[...] = both
+
     def sum_pairs(turn):
-        source, landing, sums, _, result = sum_refs(turn)
-        for target in range(chips):
-            pair_copy(turn, target).wait_recv()
         for offset in list(range(1, chips)) + [0]:
-            target = lax.rem(chip + offset, chips)
-            both = source[target * 2 + core].astype(f32) + landing[target].astype(f32)
-            if offset:
-                sums[offset] = both.astype(bf16)
-                chip_copy(turn, offset).start()
-            else:
-                result[...] = both
+            sum_pair(turn, offset)
 
     def sum_chips(turn):
         _, _, _, landing, result = sum_refs(turn)
@@ -570,8 +574,8 @@
         for head in range(head_count):
             states[head] = carried[head]
 
-    def combine(index):
-        target = lax.rem(rank + 2 + index, ranks)
+    def combine(offset, side):
+        target = lax.rem(chip + offset, chips) * 2 + side
 
         def body(step, carry):
             wide = tile_of(own)
@@ -583,6 +587,8 @@
             return carry
 
         lax.fori_loop(0, own // tile_of(own), body, 0)
+        if side is not core:
+            pair_copy(0, lax.rem(chip + offset, chips)).start()
 
     def start_pairs(turn):
         for target in range(chips):
@@ -642,11 +648,21 @@
             if who is not core:
                 start_pairs(1 + unit)
 
+    out_step = length // 4
+
+    def out_copy(index):
+        rows = pl.ds(index * out_step, out_step)
+        return pltpu.make_async_copy(result.at[rows, :], out.at[rows, :], out_sem.at[index])
+
     def last():
         scale = squares_wait(1)
-        out[...] = (
-            first[...].astype(f32) + down_total[...] * scale * last_gain[:, own_columns]
-        ).astype(bf16)
+        for index in range(4):
+            rows = slice(index * out_step, (index + 1) * out_step)
+            result[rows, :] = (
+                first[rows, :].astype(f32)
+                + down_total[rows, :] * scale[rows] * last_gain[:, own_columns]
+            ).astype(bf16)
+            out_copy(index).start()
 
     barrier = pltpu.get_barrier_semaphore()
     for way in range(2):
@@ -663,8 +679,12 @@
         barrier, there(0).astype(jnp.int32) + there(1).astype(jnp.int32) + parts - 1 + ranks - 1
     )
 
-    for unit in range(min(AHEAD, unit_count)):
-        begin(unit)
+    def lead(unit):
+        return max(0, AHEAD - unit * (AHEAD + 1) // unit_count) if FADING else AHEAD
+
+    for unit in range(unit_count):
+        if unit - lead(unit) < 0:
+            begin(unit)
     spread_start(0, block_in, rows_full)
     inputs = [
         pltpu.make_async_copy(source, target, input_sem.at[index])
@@ -696,15 +716,16 @@
     job(whole(2), 0, 0.1, lambda: [copy.wait() for copy in inputs])
     for start in range(0, chunk_count, chunk_step):
         job(whole(2), 0, 1.2, functools.partial(mix, start))
-    for index in range(ranks):
-        job(whole(3), 0, 0.7, functools.partial(combine, index))
-    job(whole(3), 0, 0.1, lambda: start_pairs(0))
-    job(-1, 1, 1.2, lambda: sum_pairs(0))
+    for offset in list(range(1, chips)) + [0]:
+        job(whole(3), 0, 0.6, functools.partial(combine, offset, 1 - core))
+        job(whole(3), 0, 0.6, functools.partial(combine, offset, core))
+    for offset in list(range(1, chips)) + [0]:
+        job(-1, 0, 0.6, functools.partial(sum_pair, 0, offset))
     job(-1, 6, 0.4, lambda: sum_chips(0))
     job(-1, 0, 1.0, lambda: squares_add(0, total, False))
     job(-1, 0, 0.1, lambda: squares_start(0))
     job(-1, 1, 0.9, make_first)
-    job(-1, 6, 0.2, lambda: spread_relay(1, first, first_full))
+    job(-1, 7, 0.2, lambda: spread_relay(1, first, first_full))
     job(-1, 1, 0.2, lambda: spread_wait(1, first, first_full))
     for start in range(0, length, norm_step):
         job(-1, 0, 0.6, functools.partial(norm_part, first_full, second_gain, start))
@@ -718,13 +739,11 @@
         squares_add(1, sum_refs(1 + unit)[4], unit > 0)
 
     for unit in range(down_cuts):
-        if unit >= 3:
-            job(-1, 0, 0.6, functools.partial(take_sum, unit - 3))
         job(last_unit(6, unit), 0, 1.2, functools.partial(down, unit))
-        if unit:
-            job(-1, 0, 0.6, functools.partial(sum_pairs, unit))
-    job(-1, 0, 0.6, functools.partial(sum_pairs, down_cuts))
-    for unit in range(max(down_cuts - 3, 0), down_cuts):
+        if unit == down_cuts - 1 and unit > 1:
+            job(-1, 0, 0.4, functools.partial(take_sum, 0))
+        job(-1, 0, 0.6, functools.partial(sum_pairs, 1 + unit))
+    for unit in range(1 if down_cuts > 2 else 0, down_cuts):
         job(-1, 0, 0.6, functools.partial(take_sum, unit))
     job(-1, 0, 0.1, lambda: squares_start(1))
     job(-1, 0, 1.0, last)
@@ -739,22 +758,32 @@
             finish(unit)
             landed[0] += 1
 
+    def first_pass(unit):
+        return unit - min(SHIFT, lead(unit))
+
+    for unit in range(unit_count):
+        if first_pass(unit) < 0:
+            pass_on(unit, 0)
     previous = 0
     slot = 0
+    arrived = {}
     for tick in range(unit_count + line - 2):
-        if tick + AHEAD < unit_count:
-            begin(tick + AHEAD)
-        for step in range(line - 1):
-            if 0 <= tick - step < unit_count:
-                pass_on(tick - step, step)
-                slot += 1
+        for unit in range(unit_count):
+            if unit - lead(unit) == tick:
+                begin(unit)
+        for step in list(range(1, line - 1)) + [0]:
+            for unit in range(unit_count):
+                if tick == (unit + step if step else first_pass(unit)):
+                    pass_on(unit, step)
+                    slot += 1
+                    if step == line - 2:
+                        arrived[unit] = slot + (LAG if units[unit][2] is None else 0)
             spent = 0.0
             while jobs:
                 needs, gap, cost, work = jobs[0]
                 if spent > 0.0 and spent + cost > STEP_BUDGET:
                     break
-                lag = LAG if needs < 0 or units[needs][2] is None else 0
-                if tick < needs + line - 1 + lag or slot < previous + gap:
+                if slot < max(previous + gap, arrived.get(needs, slot + 1 if needs >= 0 else 0)):
                     break
                 jobs.pop(0)
                 land(needs)
@@ -774,6 +803,8 @@
     for turn in range(2):
         for offset in range(1, ranks):
             squares_copy(turn, offset).wait_send()
+    for index in range(4):
+        out_copy(index).wait()
 
 
 def on_device(
@@ -865,7 +896,8 @@
         pltpu.VMEM((8, length), f32),
         pltpu.VMEM((ranks, 8, length), f32),
     ]
-    scratch += [dma((7,)), dma((2,)), dma((8, line + 1)), dma((units, line - 1))]
+    scratch += [pltpu.VMEM((length, own), bf16)]
+    scratch += [dma((4,)), dma((7,)), dma((2,)), dma((8, line + 1)), dma((units, line - 1))]
     scratch += [dma((8, line, max(parts - 1, 1))), dma((units, max(parts - 1, 1)))]
     scratch += [dma((2,))] + [dma((2, ranks))] * 2
     scratch += [dma((turns, chips))] * 4 + [dma((2, ranks))] * 2
@@ -874,7 +906,7 @@
         functools.partial(layer_kernel, (tuple(cuts), down_cuts, evened, line, parts, ranks)),
         out_shape=jax.ShapeDtypeStruct((length, own), bf16),
         in_specs=[vmem] * 10 + [anywhere] * 9,
-        out_specs=vmem,
+        out_specs=anywhere,
         scratch_shapes=scratch,
         compiler_params=pltpu.CompilerParams(
             collective_id=1, has_side_effects=True, vmem_limit_bytes=60 * 1024 * 1024

time: 159 us -> 157 us (0.987)
  Pallas kernels: 157 us -> 155 us
    pallas_call x1, Pallas kernels: 157 us -> 155 us  [on_device(): pl.pallas_call(functools.partial(layer_kernel, (tuple(cuts), down_cuts, e...]
where the time goes in v3:
time: 157 us
  Pallas kernels  155 us (99%)
  local copies, waits for them, and re-layouts  1.87 us (1%)
    pallas_call x1, Pallas kernels, on_device(): pl.pallas_call(functools.partial(layer_kernel, (tuple(cuts), down_cuts, e...  155 us

profile of v3, /device:TPU:0, one launch (start us, length us, event | category | flops | bytes accessed | tf_op | source)
XLA Modules:
  0.0 156.7 jit_solution(178807639383921089)
XLA Ops:
  0.0 154.9 %shard_map.181 = bf16[512,512]{1,0:T(8,128)(2,1)} custom-call(f32[1,2048]{1,0:T(1,128)} %bitcast.7, f32[2,256]{1,0:T(2,128)} %refs_1_.1, f32[1,2048]{1,0:T(1,128)} %bitcast.8, f32[1,2048]{1,0:T(1,128)} %bitcast.9, f32[1,2048]{1,0:T(1,128)} %bitcast.10, bf16[16,2048]{1,0:T(8,128)(2,1)} %bitcast.6, f32[16,256]{1,0:T(8,128)} %refs_6_.1, f32[1,256]{1,0:T(1,128)} %bitcast.11, ...), custom_call_target="tpu_custom_call" | custom-call | tf_op jit(solution)/shard_map/pallas_call | solution.py:905
  154.9 1.9 %copy.21 = bf16[512,512]{1,0:T(8,128)(2,1)} copy(bf16[512,512]{1,0:T(8,128)(2,1)} %shard_map.181) | data formatting | bytes 1048576

commit v4 on v3

--- a/solution.py
+++ b/solution.py
@@ -21,7 +21,9 @@
 
 AHEAD = 2
 SHIFT = 1
-FADING = False
+EARLY = 3
+EVEN_ALL = False
+FIRST_CUTS = 2
 STEP_BUDGET = 2.0
 LAG = 3
 
@@ -106,7 +108,8 @@
     units = []
     for which in range(7):
         for cut in range(cuts[which]):
-            units.append((which, cut, None))
+            if not (evened and EVEN_ALL and (which, cut) == (6, down_cuts - 1)):
+                units.append((which, cut, None))
     if evened:
         units += [(6, down_cuts - 1, half) for half in range(parts)]
     unit_count = len(units)
@@ -139,11 +142,11 @@
         shard_rows, shard_columns = shards[which].shape
         if which == 6:
             height, wide = shard_rows // parts, shard_columns // cuts[which]
-            if in_last_cut(unit):
+            if in_last_cut(unit) and not EVEN_ALL:
                 height //= 2
             row, column = half * height, cut * wide
             if fixed is not None:
-                row = shard_rows // 2 + fixed * height
+                row = shard_rows - (parts - fixed) * height
             if full:
                 column = owner * shard_columns + cut * wide
         else:
@@ -218,8 +221,9 @@
         if row == 7:
             wide = shard_columns // down_cuts
             height //= 2
+            tall = shard_rows if EVEN_ALL else height + (shard_rows // 2 if over_line else 0)
             return ref.at[
-                0 : height + (shard_rows // 2 if over_line else 0),
+                0:tall,
                 pl.ds(pl.multiple_of(owner * shard_columns + shard_columns - wide, wide), wide),
             ]
         rows = pl.ds(pl.multiple_of(part * height, height), height)
@@ -312,7 +316,7 @@
                             which, owner, line_send.at[which, owner], toward(way), True
                         ).wait_send()
 
-                    for offset in range(1, parts):
+                    for offset in range(1, 1 if which == 7 and EVEN_ALL else parts):
                         sent_part(
                             which,
                             owner,
@@ -680,7 +684,7 @@
     )
 
     def lead(unit):
-        return max(0, AHEAD - unit * (AHEAD + 1) // unit_count) if FADING else AHEAD
+        return max(AHEAD, EARLY - unit // 4)
 
     for unit in range(unit_count):
         if unit - lead(unit) < 0:
@@ -847,10 +851,10 @@
     while down_wide == own and down_cuts < cuts[6] and down_wide % (down_cuts * 2 * 128) == 0:
         down_cuts *= 2
     cuts[6] = down_cuts
-    if question_map.shape[0] % (parts * cuts[0] * 2 * 16) == 0:
+    while cuts[0] < FIRST_CUTS and question_map.shape[0] % (parts * cuts[0] * 2 * 16) == 0:
         cuts[0] *= 2
     evened = down_cuts > 1 and narrowing_map.shape[0] % (2 * parts * 16) == 0
-    units = sum(cuts) + (parts if evened else 0)
+    units = sum(cuts) + (parts - EVEN_ALL if evened else 0)
     turns = 1 + down_cuts
     down_own = own // down_cuts
     hidden_units = valve_map.shape[1]

time: 157 us -> 155 us (0.987)
  Pallas kernels: 155 us -> 153 us
    pallas_call x1, Pallas kernels: 155 us -> 153 us  [on_device(): pl.pallas_call(functools.partial(layer_kernel, (tuple(cuts), down_cuts, e...]
where the time goes in v4:
time: 155 us
  Pallas kernels  153 us (99%)
  local copies, waits for them, and re-layouts  1.87 us (1%)
    pallas_call x1, Pallas kernels, on_device(): pl.pallas_call(functools.partial(layer_kernel, (tuple(cuts), down_cuts, e...  153 us

profile of v4, /device:TPU:0, one launch (start us, length us, event | category | flops | bytes accessed | tf_op | source)
XLA Modules:
  0.0 155.0 jit_solution(15945614849856698183)
XLA Ops:
  0.0 153.1 %shard_map.181 = bf16[512,512]{1,0:T(8,128)(2,1)} custom-call(f32[1,2048]{1,0:T(1,128)} %bitcast.7, f32[2,256]{1,0:T(2,128)} %refs_1_.1, f32[1,2048]{1,0:T(1,128)} %bitcast.8, f32[1,2048]{1,0:T(1,128)} %bitcast.9, f32[1,2048]{1,0:T(1,128)} %bitcast.10, bf16[16,2048]{1,0:T(8,128)(2,1)} %bitcast.6, f32[16,256]{1,0:T(8,128)} %refs_6_.1, f32[1,256]{1,0:T(1,128)} %bitcast.11, ...), custom_call_target="tpu_custom_call" | custom-call | tf_op jit(solution)/shard_map/pallas_call | solution.py:909
  153.2 1.9 %copy.21 = bf16[512,512]{1,0:T(8,128)(2,1)} copy(bf16[512,512]{1,0:T(8,128)(2,1)} %shard_map.181) | data formatting | bytes 1048576

commit v5 on v4

--- a/solution.py
+++ b/solution.py
@@ -24,7 +24,7 @@
 EARLY = 3
 EVEN_ALL = False
 FIRST_CUTS = 2
-STEP_BUDGET = 2.0
+STEP_BUDGET = 2.3
 LAG = 3
 
 
@@ -408,8 +408,8 @@
         return remote(
             source.at[offset],
             landing.at[offset],
-            chip_send.at[turn, offset],
-            chip_recv.at[turn, offset],
+            chip_send.at[turn, offset - 1],
+            chip_recv.at[turn, offset - 1],
             {"tp": lax.rem(chip + offset, chips) * 2 + core},
         )
 
@@ -445,8 +445,8 @@
         return remote(
             source,
             landing.at[offset],
-            squares_send.at[turn, offset],
-            squares_recv.at[turn, offset],
+            squares_send.at[turn, offset - 1],
+            squares_recv.at[turn, offset - 1],
             {"tp": rank_at(offset)},
         )
 
@@ -904,7 +904,7 @@
     scratch += [dma((4,)), dma((7,)), dma((2,)), dma((8, line + 1)), dma((units, line - 1))]
     scratch += [dma((8, line, max(parts - 1, 1))), dma((units, max(parts - 1, 1)))]
     scratch += [dma((2,))] + [dma((2, ranks))] * 2
-    scratch += [dma((turns, chips))] * 4 + [dma((2, ranks))] * 2
+    scratch += [dma((turns, chips))] * 2 + [dma((turns, max(chips - 1, 1)))] * 2 + [dma((2, ranks - 1))] * 2
     vmem, anywhere = pl.BlockSpec(memory_space=pltpu.VMEM), pl.BlockSpec(memory_space=pl.ANY)
     return pl.pallas_call(
         functools.partial(layer_kernel, (tuple(cuts), down_cuts, evened, line, parts, ranks)),

time: 155 us -> 155 us (level)
  no operation moved by 1% of the time
where the time goes in v5:
time: 155 us
  Pallas kernels  153 us (99%)
  local copies, waits for them, and re-layouts  1.87 us (1%)
    pallas_call x1, Pallas kernels, on_device(): pl.pallas_call(functools.partial(layer_kernel, (tuple(cuts), down_cuts, e...  153 us

profile of v5, /device:TPU:0, one launch (start us, length us, event | category | flops | bytes accessed | tf_op | source)
XLA Modules:
  0.0 154.9 jit_solution(16265615904590065903)
XLA Ops:
  0.0 153.0 %shard_map.181 = bf16[512,512]{1,0:T(8,128)(2,1)} custom-call(f32[1,2048]{1,0:T(1,128)} %bitcast.7, f32[2,256]{1,0:T(2,128)} %refs_1_.1, f32[1,2048]{1,0:T(1,128)} %bitcast.8, f32[1,2048]{1,0:T(1,128)} %bitcast.9, f32[1,2048]{1,0:T(1,128)} %bitcast.10, bf16[16,2048]{1,0:T(8,128)(2,1)} %bitcast.6, f32[16,256]{1,0:T(8,128)} %refs_6_.1, f32[1,256]{1,0:T(1,128)} %bitcast.11, ...), custom_call_target="tpu_custom_call" | custom-call | tf_op jit(solution)/shard_map/pallas_call | solution.py:909
  153.0 1.9 %copy.21 = bf16[512,512]{1,0:T(8,128)(2,1)} copy(bf16[512,512]{1,0:T(8,128)(2,1)} %shard_map.181) | data formatting | bytes 1048576
